TPU v7x, 32 devices: a whole 2x2x4 slice. The times are simulated.
32 devices in a mesh: ep: 8 (over z, core), tp: 4 (over y, x).
Axes of the slice: x: 2, y: 2, z: 4, core: 2. Of those that a mesh axis runs over, the one named last changes fastest.
Arguments:
- queries: bfloat16 [1024, 4096], P('ep', 'tp'), may hold values from -32 to 32
- keys: bfloat16 [1024, 2048], P('ep', 'tp'), may hold values from -32 to 32
- values: bfloat16 [1024, 2048], P('ep', 'tp'), may hold values from -6 to 6
- query_gain: float32 [128], replicated, may hold values from 1 to 6
- key_gain: float32 [128], replicated, may hold values from 1 to 6
- out_weight: bfloat16 [4096, 2048], P('tp'), may hold values from -0.75 to 0.75
- expert_input: bfloat16 [1024, 2048], P('ep'), may hold values from -64 to 64
- norm_gain: float32 [2048], replicated, may hold values from 0.1 to 1.9
- routes: int32 [1024, 2], P('ep'), may hold values from 0 to 7, all different within a row; in each aligned block of 128 rows (0 to 127, 128 to 255, ...) at most 40 rows name the same one
- route_logits: float32 [1024, 2], P('ep'), may hold values from -6 to 6
- gate_weight: bfloat16 [8, 2048, 2816], P('ep', None, 'tp'), may hold values from -0.125 to 0.125
- up_weight: bfloat16 [8, 2048, 2816], P('ep', None, 'tp'), may hold values from -0.125 to 0.125
- down_weight: bfloat16 [8, 2816, 2048], P('ep', 'tp'), may hold values from -0.109375 to 0.109375
Outputs:
- mixed: bfloat16 [1024, 2048], P(('ep', 'tp'))
- expert_out: bfloat16 [1024, 2048], P('ep', 'tp')
Inputs may be any that keep to these rules, and one draw needn't show every extreme that they name: `routes`: A token's 2 experts differ. Among the 128 tokens of one index of ep (aligned blocks), no expert is named by more than 40 tokens, a bound that some block reaches.
All inputs are finite; a program needn't handle non-finite values.
Results may differ from a plain program's by a relative error of at most 0.015.
The roundings to bfloat16 on the way count: a program that leaves them out, or rounds other values in their place, can miss the bound.
Values may be sent and summed in bfloat16 or wider, within the bound.
A program may use at most 64 MiB of HBM per device.

v0:
```python
import functools
import jax
import jax.numpy as jnp
import numpy as np
from jax import lax
from jax.experimental import pallas as pl
from jax.experimental.pallas import tpu as pltpu
from jax.sharding import PartitionSpec as P

GRID_W = 64


def rope_tables(count, offset, head_dim):
    pos = offset + lax.iota(jnp.int32, count)
    grid_row = (pos // GRID_W).astype(jnp.float32)
    grid_col = (pos % GRID_W).astype(jnp.float32)
    quarter = head_dim // 4
    inverse = 10000.0 ** (-jnp.arange(quarter, dtype=jnp.float32) / quarter)
    angles = jnp.concatenate([grid_row[:, None] * inverse, grid_col[:, None] * inverse], axis=-1)
    return (jnp.cos(angles), jnp.sin(angles))


def norm_rotate(x, gain, cosine, sine):
    count, number, head_dim = x.shape
    y = x * lax.rsqrt(jnp.mean(x * x, axis=-1, keepdims=True) + 1e-06) * gain
    pairs = y.reshape(count, number, head_dim // 2, 2)
    first, second = (pairs[..., 0], pairs[..., 1])
    cos_b = cosine[:, None, :]
    sin_b = sine[:, None, :]
    turned = jnp.stack([first * cos_b - second * sin_b, first * sin_b + second * cos_b], axis=-1)
    return turned.reshape(count, number, head_dim).astype(jnp.bfloat16)


def key_block_size(length, shard_rows):
    if length <= 2048:
        return length
    shards = length // shard_rows
    most = max(1, 2048 // shard_rows)
    best = 1
    for count in range(1, most + 1):
        if shards % count == 0:
            best = count
    return best * shard_rows


def local(
    queries,
    keys,
    values,
    query_gain,
    key_gain,
    out_weight,
    expert_input,
    norm_gain,
    routes,
    route_logits,
    gate_weight,
    up_weight,
    down_weight,
):
    tokens_here = queries.shape[0]
    head_dim = query_gain.shape[0]
    heads_here = queries.shape[1] // head_dim
    kv_here = keys.shape[1] // head_dim
    group = heads_here // kv_here
    offset = lax.axis_index("ep") * tokens_here
    cosine, sine = rope_tables(tokens_here, offset, head_dim)
    q_rot = norm_rotate(
        queries.astype(jnp.float32).reshape(tokens_here, heads_here, head_dim),
        query_gain,
        cosine,
        sine,
    )
    k_rot = norm_rotate(
        keys.astype(jnp.float32).reshape(tokens_here, kv_here, head_dim), key_gain, cosine, sine
    ).reshape(tokens_here, kv_here * head_dim)
    q_grouped = q_rot.reshape(tokens_here, kv_here, group, head_dim).transpose(1, 2, 0, 3)
    q_grouped = q_grouped.reshape(kv_here, group * tokens_here, head_dim)
    query_rows = group * tokens_here
    scale = head_dim ** (-0.5)
    start_state = (
        jnp.full((kv_here, query_rows), -1e30, jnp.float32),
        jnp.zeros((kv_here, query_rows), jnp.float32),
        jnp.zeros((kv_here, query_rows, head_dim), jnp.float32),
    )
    key_piece = lax.all_gather(k_rot, "ep", axis=0, tiled=True)
    value_piece = lax.all_gather(values, "ep", axis=0, tiled=True)
    length = key_piece.shape[0]
    block = key_block_size(length, tokens_here)
    key_blocks = key_piece.reshape(length // block, block, kv_here, head_dim)
    value_blocks = value_piece.reshape(length // block, block, kv_here, head_dim)

    def step(state, blocks):
        running_max, running_total, running_sum = state
        key_block, value_block = blocks
        scores = (
            jnp.einsum("kqd,lkd->kql", q_grouped, key_block, preferred_element_type=jnp.float32)
            * scale
        )
        new_max = jnp.maximum(running_max, jnp.max(scores, axis=-1))
        factor = jnp.exp(running_max - new_max)
        weights = jnp.exp(scores - new_max[..., None])
        new_total = running_total * factor + jnp.sum(weights, axis=-1)
        new_sum = running_sum * factor[..., None] + jnp.einsum(
            "kql,lkd->kqd",
            weights.astype(jnp.bfloat16),
            value_block,
            preferred_element_type=jnp.float32,
        )
        return ((new_max, new_total, new_sum), None)

    result, _ = lax.scan(step, start_state, (key_blocks, value_blocks))
    final_max, final_total, final_sum = result
    attended = (final_sum / final_total[..., None]).astype(jnp.bfloat16)
    attended = attended.reshape(kv_here, group, tokens_here, head_dim).transpose(2, 0, 1, 3)
    attended = attended.reshape(tokens_here, heads_here * head_dim)
    summed = lax.psum_scatter(
        jnp.dot(attended, out_weight, preferred_element_type=jnp.float32).astype(jnp.bfloat16),
        "tp",
        scatter_dimension=0,
        tiled=True,
    ).astype(jnp.float32)
    mixed = summed.astype(jnp.bfloat16)
    expert_tokens_here, width = expert_input.shape
    n_ep = lax.axis_size("ep")
    top = routes.shape[1]
    capacity = expert_tokens_here * top // n_ep * 5 // 4
    x = expert_input.astype(jnp.float32)
    normed = (x * lax.rsqrt(jnp.mean(x * x, axis=-1, keepdims=True) + 1e-06) * norm_gain).astype(
        jnp.bfloat16
    )
    expert_ids = routes.reshape(-1)
    onehot = (expert_ids[:, None] == lax.iota(jnp.int32, n_ep)[None, :]).astype(jnp.int32)
    before = jnp.cumsum(onehot, axis=0) - onehot
    slot = jnp.sum(before * onehot, axis=1)
    target = expert_ids * capacity + slot
    owner_row = lax.iota(jnp.int32, expert_tokens_here * top) // top
    w_gate = gate_weight[0]
    w_up = up_weight[0]
    w_down = down_weight[0]
    columns = normed.shape[1]
    filled = jnp.zeros((n_ep * capacity, columns), jnp.bfloat16).at[target].set(normed[owner_row])
    arrived = lax.all_to_all(
        filled.reshape(n_ep, capacity, columns), "ep", split_axis=0, concat_axis=0, tiled=True
    )
    sources, slots, work_columns = arrived.shape
    flat = arrived.reshape(sources * slots, work_columns)
    gate = jnp.dot(flat, w_gate, preferred_element_type=jnp.float32)
    upper = jnp.dot(flat, w_up, preferred_element_type=jnp.float32)
    hidden = (jax.nn.silu(gate) * upper).astype(jnp.bfloat16)
    partial_out = jnp.dot(hidden, w_down, preferred_element_type=jnp.float32)
    summed = lax.psum_scatter(
        partial_out.reshape(sources, slots, width).astype(jnp.bfloat16),
        "tp",
        scatter_dimension=2,
        tiled=True,
    ).astype(jnp.float32)
    returned = lax.all_to_all(
        summed.astype(jnp.bfloat16), "ep", split_axis=0, concat_axis=0, tiled=True
    )
    picked = returned.reshape(n_ep * capacity, -1)[target].reshape(expert_tokens_here, top, -1)
    route_weight = jax.nn.sigmoid(route_logits - route_logits[:, ::-1])
    combined = jnp.sum(route_weight[..., None] * picked.astype(jnp.float32), axis=1)
    expert_out = combined.astype(jnp.bfloat16)
    return (mixed, expert_out)


MESH = pl.DeviceIdType.MESH


def rope_constants(length, head_dim):
    pos = np.arange(length)
    quarter = head_dim // 4
    inverse = (np.float32(10000.0) ** (-np.arange(quarter, dtype=np.float32) / np.float32(quarter))).astype(np.float32)
    grid_row = (pos // GRID_W).astype(np.float32)
    grid_col = (pos % GRID_W).astype(np.float32)
    angles = np.concatenate([grid_row[:, None] * inverse, grid_col[:, None] * inverse], axis=-1)
    cosine = np.repeat(np.cos(angles), 2, axis=-1).astype(np.float32)
    sine = np.repeat(np.sin(angles), 2, axis=-1).astype(np.float32)
    sine[:, 0::2] *= -1.0
    return np.stack([cosine, sine])


def fused(
    dims,
    q_hbm,
    k_hbm,
    v_hbm,
    qg_ref,
    kg_ref,
    wo_hbm,
    x_hbm,
    ng_ref,
    rt_ref,
    lg_ref,
    wg_hbm,
    wu_hbm,
    wd_hbm,
    rope_hbm,
    mixed_hbm,
    eout_hbm,
    mixed_ref,
    eout_ref,
    q_ref,
    k_ref,
    x_ref,
    amax,
    atot,
    asum,
    wo,
    wg,
    wu,
    wd,
    rope,
    disp,
    xq,
    gacc,
    uacc,
    hid,
    part,
    rdiag,
    rsx,
    rsy,
    back,
    ret,
    kv,
    qrot,
    att,
    mpart,
    mrecv,
    wsem,
    zs,
    zr,
    axs,
    axr,
    ays,
    ayr,
    afs,
    afr,
    kvs,
    kvu,
    kvd,
    kvr,
    rds,
    rdr,
    rxs,
    rxr,
    rys,
    ryr,
    bs,
    br,
    ms,
    mr,
):
    n_ep, cap, head_dim, kv_here, group = dims
    f32, bf16 = jnp.float32, jnp.bfloat16
    chips = n_ep // 2
    me = lax.axis_index("ep")
    t = lax.axis_index("tp")
    tx = t + 1 - 2 * (t % 2)
    ty = (t + 2) % 4
    td = 3 - t
    z = me // 2
    core = me % 2
    mate = 2 * z + 1 - core
    if chips == 4:
        inner = (z == 1) | (z == 2)
        across = (z + 2) % 4
        mirror = 3 - z
        near = [z + 1 - 2 * (z % 2), jnp.where(inner, mirror, across), jnp.where(inner, across, mirror)]
    else:
        near = [(z + k) % chips for k in range(1, chips)]
    order = [me, mate]
    for chip in near:
        order += [2 * chip + core, 2 * chip + 1 - core]
    far_first = order[::-1]
    tokens = x_ref.shape[0]
    slab = disp.shape[2]
    rows = n_ep * cap

    barrier = pltpu.get_barrier_semaphore()
    for d in range(1, n_ep):
        pl.semaphore_signal(barrier, inc=1, device_id={"ep": (me + d) % n_ep}, device_id_type=MESH)
    for peer in (tx, ty, td):
        pl.semaphore_signal(barrier, inc=1, device_id={"tp": peer}, device_id_type=MESH)

    x_load = pltpu.make_async_copy(x_hbm, x_ref, wsem.at[5])
    x_load.start()
    k_load = pltpu.make_async_copy(k_hbm, k_ref, wsem.at[6])
    k_load.start()
    rope_copy = pltpu.make_async_copy(
        rope_hbm.at[:, pl.ds(pl.multiple_of(me * tokens, tokens), tokens), :], rope, wsem.at[0]
    )
    rope_copy.start()
    v_load = pltpu.make_async_copy(v_hbm, kv.at[me, 1], wsem.at[7])
    v_load.start()
    q_load = pltpu.make_async_copy(q_hbm, q_ref, wsem.at[8])
    q_load.start()
    loads = [
        pltpu.make_async_copy(wg_hbm.at[0], wg, wsem.at[1]),
        pltpu.make_async_copy(wu_hbm.at[0], wu, wsem.at[2]),
        pltpu.make_async_copy(wd_hbm.at[0], wd, wsem.at[3]),
        pltpu.make_async_copy(wo_hbm, wo, wsem.at[4]),
    ]
    for load in loads:
        load.start()

    wide = (tokens, tokens)
    lane = lax.broadcasted_iota(jnp.int32, wide, 1)
    sub = lax.broadcasted_iota(jnp.int32, wide, 0)
    routed = (sub == rt_ref[0:1, :]) | (sub == rt_ref[1:2, :])
    named_t = jnp.where(routed, 1.0, 0.0)
    named = named_t.T
    ids = rt_ref[...].astype(f32)
    logits = lg_ref[...]
    stacked = jnp.where(
        sub == 0,
        ids[0:1, :],
        jnp.where(sub == 1, ids[1:2, :], jnp.where(sub == 2, logits[0:1, :], logits[1:2, :])),
    )
    columns = stacked.T
    r0 = columns[:, 0:1].astype(jnp.int32)
    r1 = columns[:, 1:2].astype(jnp.int32)
    upper = jnp.where(sub < lane, 1.0, 0.0).astype(bf16)
    lower = jnp.where(lane < sub, 1.0, 0.0).astype(bf16)
    rank_t = jnp.dot(named_t.astype(bf16), upper, preferred_element_type=f32)
    rank = jnp.dot(lower, named.astype(bf16), preferred_element_type=f32)
    slot_iota = lax.broadcasted_iota(jnp.int32, (cap, tokens), 0).astype(f32)
    picks = [
        jnp.where((slot_iota == rank_t[e : e + 1, :]) & (named_t[e : e + 1, :] > 0.5), 1.0, 0.0)
        for e in range(n_ep)
    ]
    pick = jnp.concatenate(picks, axis=0).astype(bf16)

    x_load.wait()
    x = x_ref[...].astype(f32)
    inv = lax.rsqrt(jnp.mean(x * x, axis=-1, keepdims=True) + 1e-06)
    cols = pl.ds(pl.multiple_of(t * slab, slab), slab)
    normed = (x_ref[:, cols].astype(f32) * inv * ng_ref[:, cols]).astype(bf16)
    sent = jnp.dot(pick, normed, preferred_element_type=f32)
    for e in range(n_ep):
        disp[e] = sent[e * cap : (e + 1) * cap].astype(bf16)
    xq[t, me] = disp[me]

    pl.semaphore_wait(barrier, n_ep - 1 + 3)

    def remote(a, b, s, r, **where):
        return pltpu.make_async_remote_copy(
            src_ref=a, dst_ref=b, send_sem=s, recv_sem=r, device_id=where, device_id_type=MESH
        )

    def z_copy(d):
        e = order[d]
        return remote(disp.at[e], xq.at[t, me], zs.at[e], zr.at[me], ep=e)

    for d in range(1, n_ep):
        z_copy(d).start()

    rope_copy.wait()
    cos = rope[0]
    sin = rope[1]
    even = lax.broadcasted_iota(jnp.int32, (tokens, head_dim), 1) % 2 == 0

    def turn(piece, gain):
        a = piece.astype(f32)
        y = a * lax.rsqrt(jnp.mean(a * a, axis=-1, keepdims=True) + 1e-06) * gain
        other = jnp.where(even, pltpu.roll(y, head_dim - 1, 1), pltpu.roll(y, 1, 1))
        return (y * cos + other * sin).astype(bf16)

    k_load.wait()
    for g in range(kv_here):
        at = slice(g * head_dim, (g + 1) * head_dim)
        kv[me, 0, :, at] = turn(k_ref[:, at], kg_ref[...])
    v_load.wait()
    q_load.wait()

    for h in range(kv_here * group):
        at = slice(h * head_dim, (h + 1) * head_dim)
        qrot[h] = turn(q_ref[:, at], qg_ref[...])

    def x_copy(s):
        return remote(xq.at[t, s], xq.at[t, s], axs.at[s], axr.at[s], tp=tx)

    def y_copy(s):
        return remote(xq.at[t, s], xq.at[t, s], ays.at[s], ayr.at[s], tp=ty)

    def wait_in(ref, sem):
        pltpu.make_async_remote_copy(
            src_ref=ref, dst_ref=ref, send_sem=zs.at[0], recv_sem=sem, device_id={"tp": tx}, device_id_type=MESH
        ).wait_recv()

    def on_copy(s, q, to):
        return remote(xq.at[q, s], xq.at[q, s], afs.at[s], afr.at[s], tp=to)

    for d in range(n_ep):
        s = order[d]
        if d > 0:
            wait_in(xq.at[t, s], zr.at[s])
        x_copy(s).start()
        y_copy(s).start()

    def kv_copy(block, to, sem):
        return remote(kv.at[block], kv.at[block], sem, kvr.at[block], ep=to)

    def lane_of(chip):
        return 2 * chip + core

    def own_kv(act):
        for k in (2, 1):
            if k < chips:

                @pl.when(z + k < chips)
                def _():
                    act(kv_copy(me, lane_of(z + k), kvu.at[k]))

                @pl.when(z >= k)
                def _():
                    act(kv_copy(me, lane_of(z - k), kvd.at[k]))

        act(kv_copy(me, mate, kvs.at[me]))

    def forward_kv(k, act, arrive):
        @pl.when((z >= k) & (z + 1 < chips))
        def _():
            block = lane_of(z - k)
            if arrive:
                wait_in(kv.at[block], kvr.at[block])
            act(kv_copy(block, mate, kvs.at[block]))
            act(kv_copy(block, lane_of(z + 1), kvu.at[k + 1]))

        @pl.when((z + k < chips) & (z >= 1))
        def _():
            block = lane_of(z + k)
            if arrive:
                wait_in(kv.at[block], kvr.at[block])
            act(kv_copy(block, mate, kvs.at[block]))
            act(kv_copy(block, lane_of(z - 1), kvd.at[k + 1]))

    def relay_kv(k, act, arrive):
        below, above = z >= k, z + k < chips
        if k == 2:
            below, above = below & (z + 1 >= chips), above & (z < 1)

        @pl.when(below)
        def _():
            block = lane_of(z - k)
            if arrive:
                wait_in(kv.at[block], kvr.at[block])
            act(kv_copy(block, mate, kvs.at[block]))

        @pl.when(above)
        def _():
            block = lane_of(z + k)
            if arrive:
                wait_in(kv.at[block], kvr.at[block])
            act(kv_copy(block, mate, kvs.at[block]))

    own_kv(lambda c: c.start())
    loads[0].wait()
    loads[1].wait()

    def gate_up(q, first):
        block = xq[q].astype(f32).reshape(rows, slab).astype(bf16)
        at = pl.ds(pl.multiple_of(q * slab, slab), slab)
        g = lax.dot_general(block, wg[:, at], (((1,), (1,)), ((), ())), preferred_element_type=f32)
        u = lax.dot_general(block, wu[:, at], (((1,), (1,)), ((), ())), preferred_element_type=f32)
        if first:
            gacc[...] = g
            uacc[...] = u
        else:
            gacc[...] += g
            uacc[...] += u

    gate_up(t, True)
    for i in range(n_ep):
        s = order[i]
        if i % 2 == 0:
            wait_in(xq.at[tx, s], axr.at[s])
            on_copy(s, tx, ty).start()
        else:
            wait_in(xq.at[ty, s], ayr.at[s])
            on_copy(s, ty, tx).start()
    for i in range(n_ep):
        s = order[i]
        if i % 2 == 0:
            wait_in(xq.at[ty, s], ayr.at[s])
        else:
            wait_in(xq.at[tx, s], axr.at[s])
    gate_up(tx, False)
    gate_up(ty, False)
    for i in range(n_ep):
        wait_in(xq.at[td, order[i]], afr.at[order[i]])
    gate_up(td, False)
    gate = gacc[...]
    hid[...] = (gate / (1.0 + jnp.exp(-gate)) * uacc[...]).astype(bf16)
    loads[2].wait()

    def down(q):
        at = pl.ds(pl.multiple_of(q * slab, slab), slab)
        out = jnp.dot(hid[...], wd[:, at], preferred_element_type=f32)
        for s in range(n_ep):
            part[q, s] = out[s * cap : (s + 1) * cap].astype(bf16)

    def far_copy(i):
        s = far_first[i]
        to = tx if i % 2 == 0 else ty
        return remote(part.at[td, s], rdiag.at[s], rds.at[s], rdr.at[s], tp=to)

    def rx_copy(s):
        return remote(part.at[tx, s], rsx.at[s], rxs.at[s], rxr.at[s], tp=tx)

    def ry_copy(s):
        return remote(part.at[ty, s], rsy.at[s], rys.at[s], ryr.at[s], tp=ty)

    down(td)
    for i in range(n_ep):
        far_copy(i).start()
    down(tx)
    for i in range(0, n_ep, 2):
        rx_copy(far_first[i]).start()
    down(ty)
    for i in range(1, n_ep, 2):
        ry_copy(far_first[i]).start()
    down(t)
    forward_kv(2, lambda c: c.start(), True)
    for i in range(n_ep):
        s = far_first[i]
        wait_in(rdiag.at[s], rdr.at[s])
        if i % 2 == 0:
            part[ty, s] = (part[ty, s].astype(f32) + rdiag[s].astype(f32)).astype(bf16)
            ry_copy(s).start()
        else:
            part[tx, s] = (part[tx, s].astype(f32) + rdiag[s].astype(f32)).astype(bf16)
            rx_copy(s).start()
    relay_kv(1, lambda c: c.start(), True)
    relay_kv(2, lambda c: c.start(), True)
    last = jnp.where(z * 2 < chips, chips - 1, 0)
    first_chip = jnp.where(z * 2 < chips, 0, 1)
    scale = head_dim ** (-0.5)

    def scores_of(g, start, count):
        at = slice(g * head_dim, (g + 1) * head_dim)
        blocks = pl.ds(2 * start, 2 * count)
        keys = kv[blocks, 0, :, at].reshape(2 * count * tokens, head_dim)
        vals = kv[blocks, 1, :, at].reshape(2 * count * tokens, head_dim)
        q2 = qrot[g * group : (g + 1) * group].reshape(group * tokens, head_dim)
        s = lax.dot_general(q2, keys, (((1,), (1,)), ((), ())), preferred_element_type=f32)
        return s * scale, vals

    for k in range(chips - 1):
        block = 2 * (first_chip + k) + 1 - core
        wait_in(kv.at[block], kvr.at[block])
    for g in range(kv_here):
        scores, vals = scores_of(g, first_chip, chips - 1)
        peak = jnp.max(scores, axis=-1, keepdims=True)
        p = jnp.exp(scores - peak)
        amax[g] = peak
        atot[g] = jnp.sum(p, axis=-1, keepdims=True)
        asum[g] = jnp.dot(p.astype(bf16), vals, preferred_element_type=f32)

    def back_copy(s):
        return remote(back.at[s], ret.at[me], bs.at[s], br.at[me], ep=s)

    for i in range(n_ep):
        s = far_first[i]
        wait_in(rsx.at[s], rxr.at[s])
        wait_in(rsy.at[s], ryr.at[s])
        out = (part[t, s].astype(f32) + rsx[s].astype(f32) + rsy[s].astype(f32)).astype(bf16)
        if i < n_ep - 1:
            back[s] = out
            back_copy(s).start()
        else:
            ret[s] = out

    relay_kv(3, lambda c: c.start(), True)
    last_block = 2 * last + 1 - core
    wait_in(kv.at[last_block], kvr.at[last_block])
    for g in range(kv_here):
        scores, vals = scores_of(g, last, 1)
        peak = jnp.maximum(amax[g], jnp.max(scores, axis=-1, keepdims=True))
        p = jnp.exp(scores - peak)
        factor = jnp.exp(amax[g] - peak)
        total = atot[g] * factor + jnp.sum(p, axis=-1, keepdims=True)
        out = (asum[g] * factor + jnp.dot(p.astype(bf16), vals, preferred_element_type=f32)) / total
        for r in range(group):
            h = g * group + r
            att[:, h * head_dim : (h + 1) * head_dim] = out[r * tokens : (r + 1) * tokens].astype(bf16)
    loads[3].wait()
    share = tokens // 4
    width = wo.shape[1]
    chunk = width // 4

    def m_copy(i, c):
        to = (td, tx, ty)[i]
        return remote(mpart.at[c, to], mrecv.at[c, i], ms.at[c, i], mr.at[c, i], tp=to)

    for c in range(4):
        out = jnp.dot(att[...], wo[:, c * chunk : (c + 1) * chunk], preferred_element_type=f32)
        for j in range(4):
            mpart[c, j] = out[j * share : (j + 1) * share].astype(bf16)
        for i in range(3):
            m_copy(i, c).start()

    rank_lane = lane
    total_lane = lax.broadcasted_iota(jnp.int32, (tokens, rows), 1)

    def chosen(r):
        slot = jnp.sum(jnp.where(rank_lane == r, rank, 0.0), axis=-1, keepdims=True)
        target = r * cap + slot.astype(jnp.int32)
        return jnp.where(total_lane == target, 1.0, 0.0).astype(bf16)

    c0 = chosen(r0)
    c1 = chosen(r1)
    l0 = columns[:, 2:3]
    l1 = columns[:, 3:4]
    w0 = jax.nn.sigmoid(l0 - l1)
    w1 = jax.nn.sigmoid(l1 - l0)
    for d in range(1, n_ep):
        e = (me + d) % n_ep
        wait_in(ret.at[e], br.at[e])
    results = ret[...].astype(f32).reshape(rows, slab).astype(bf16)
    first = jnp.dot(c0, results, preferred_element_type=f32)
    second = jnp.dot(c1, results, preferred_element_type=f32)
    eout_ref[...] = (w0 * first + w1 * second).astype(bf16)
    e_store = pltpu.make_async_copy(eout_ref, eout_hbm, wsem.at[9])
    e_store.start()

    def m_store(c):
        at = slice(c * chunk, (c + 1) * chunk)
        return pltpu.make_async_copy(mixed_ref.at[c], mixed_hbm.at[:, at], wsem.at[10 + c])

    for c in range(4):
        summed = mpart[c, t].astype(f32)
        for i in range(3):
            wait_in(mrecv.at[c, i], mr.at[c, i])
            summed = summed + mrecv[c, i].astype(f32)
        mixed_ref[c] = summed.astype(bf16)
        m_store(c).start()

    for d in range(1, n_ep):
        z_copy(d).wait_send()
    own_kv(lambda c: c.wait_send())
    forward_kv(2, lambda c: c.wait_send(), False)
    for k in range(1, chips):
        relay_kv(k, lambda c: c.wait_send(), False)
    for i in range(n_ep):
        s = order[i]
        x_copy(s).wait_send()
        y_copy(s).wait_send()
        on_copy(s, tx if i % 2 == 0 else ty, ty if i % 2 == 0 else tx).wait_send()
        far_copy(i).wait_send()
        rx_copy(s).wait_send()
        ry_copy(s).wait_send()
        if i > 0:
            back_copy(s).wait_send()

    for c in range(4):
        for i in range(3):
            m_copy(i, c).wait_send()
    e_store.wait()
    for c in range(4):
        m_store(c).wait()


def hand_over(a_ref, b_ref, a_out, b_out):
    a_out[...] = a_ref[...]
    b_out[...] = b_ref[...]


def kernel_form(
    queries,
    keys,
    values,
    query_gain,
    key_gain,
    out_weight,
    expert_input,
    norm_gain,
    routes,
    route_logits,
    gate_weight,
    up_weight,
    down_weight,
):
    bf16, f32 = jnp.bfloat16, jnp.float32
    n_ep = lax.axis_size("ep")
    tokens = queries.shape[0]
    head_dim = query_gain.shape[0]
    heads = queries.shape[1] // head_dim
    kv_here = keys.shape[1] // head_dim
    width = expert_input.shape[1]
    n_tp = lax.axis_size("tp")
    slab = width // n_tp
    cap = tokens * routes.shape[1] // n_ep * 5 // 4
    rows = n_ep * cap
    ff = gate_weight.shape[2]
    share = tokens // n_tp
    table = jnp.asarray(rope_constants(tokens * n_ep, head_dim))
    vmem = pl.BlockSpec(memory_space=pltpu.VMEM)
    hbm = pl.BlockSpec(memory_space=pl.ANY)
    piece = (n_ep, cap, slab)
    dma = pltpu.SemaphoreType.DMA
    dims = (n_ep, cap, head_dim, kv_here, heads // kv_here)
    outs = pl.pallas_call(
        functools.partial(fused, dims),
        name="fused",
        out_shape=(
            jax.ShapeDtypeStruct((share, out_weight.shape[1]), bf16),
            jax.ShapeDtypeStruct((tokens, slab), bf16),
        ),
        in_specs=[hbm, hbm, hbm, vmem, vmem, hbm, hbm, vmem, vmem, vmem, hbm, hbm, hbm, hbm],
        out_specs=(hbm, hbm),
        scratch_shapes=[
            pltpu.VMEM((4, share, out_weight.shape[1] // 4), bf16),
            pltpu.VMEM((tokens, slab), bf16),
            pltpu.VMEM(queries.shape, bf16),
            pltpu.VMEM(keys.shape, bf16),
            pltpu.VMEM(expert_input.shape, bf16),
            pltpu.VMEM((kv_here, heads // kv_here * tokens, 1), f32),
            pltpu.VMEM((kv_here, heads // kv_here * tokens, 1), f32),
            pltpu.VMEM((kv_here, heads // kv_here * tokens, head_dim), f32),
            pltpu.VMEM(out_weight.shape, bf16),
            pltpu.VMEM((ff, width), bf16),
            pltpu.VMEM((ff, width), bf16),
            pltpu.VMEM(down_weight.shape[1:], bf16),
            pltpu.VMEM((2, tokens, head_dim), f32),
            pltpu.VMEM(piece, bf16),
            pltpu.VMEM((n_tp,) + piece, bf16),
            pltpu.VMEM((rows, ff), f32),
            pltpu.VMEM((rows, ff), f32),
            pltpu.VMEM((rows, ff), bf16),
            pltpu.VMEM((n_tp,) + piece, bf16),
            pltpu.VMEM(piece, bf16),
            pltpu.VMEM(piece, bf16),
            pltpu.VMEM(piece, bf16),
            pltpu.VMEM(piece, bf16),
            pltpu.VMEM(piece, bf16),
            pltpu.VMEM((n_ep, 2, tokens, kv_here * head_dim), bf16),
            pltpu.VMEM((heads, tokens, head_dim), bf16),
            pltpu.VMEM((tokens, heads * head_dim), bf16),
            pltpu.VMEM((4, n_tp, share, out_weight.shape[1] // 4), bf16),
            pltpu.VMEM((4, 3, share, out_weight.shape[1] // 4), bf16),
            dma((14,)),
        ]
        + [dma((n_ep,))] * 20
        + [dma((4, 3))] * 2,
        compiler_params=pltpu.CompilerParams(
            collective_id=0, has_side_effects=True, vmem_limit_bytes=60 * 1024 * 1024
        ),
    )(
        queries,
        keys,
        values,
        query_gain.reshape(1, -1),
        key_gain.reshape(1, -1),
        out_weight,
        expert_input,
        norm_gain.reshape(1, -1),
        routes.T,
        route_logits.T,
        jnp.swapaxes(gate_weight, 1, 2),
        jnp.swapaxes(up_weight, 1, 2),
        down_weight,
        table,
    )
    return pl.pallas_call(
        hand_over,
        name="hand_over",
        out_shape=tuple(jax.ShapeDtypeStruct(o.shape, o.dtype) for o in outs),
        in_specs=[vmem, vmem],
        out_specs=(vmem, vmem),
    )(*outs)


def dispatch_form(mesh, *args):
    queries, routes = args[0], args[8]
    tokens = queries.shape[0]
    n_ep, n_tp = mesh.shape["ep"], mesh.shape["tp"]
    cap = tokens * routes.shape[1] // n_ep * 5 // 4
    same = args[6].shape[0] == tokens and tokens % 128 == 0
    fits = n_tp == 4 and n_ep == 8 and cap % 8 == 0
    if same and fits and routes.shape[1] == 2 and tokens == 128:
        return kernel_form(*args)
    return local(*args)


def solution(mesh):
    placed = (
        P("ep", "tp"),
        P("ep", "tp"),
        P("ep", "tp"),
        P(),
        P(),
        P("tp", None),
        P("ep", None),
        P(),
        P("ep", None),
        P("ep", None),
        P("ep", None, "tp"),
        P("ep", None, "tp"),
        P("ep", "tp", None),
    )
    return jax.shard_map(
        functools.partial(dispatch_form, mesh),
        mesh=mesh,
        in_specs=placed,
        out_specs=(P(("ep", "tp"), None), P("ep", "tp")),
        check_vma=False,
    )
```

profile of v0, /device:TPU:0, one launch (start us, length us, event | category | flops | bytes accessed | tf_op | source)
XLA Modules:
  0.0 51.0 jit_solution(8811285945347253561)
XLA Ops:
  0.6 48.7 %fused.1 = (bf16[32,2048]{1,0:T(8,128)(2,1)}, bf16[128,512]{1,0:T(8,128)(2,1)}) custom-call(bf16[128,1024]{1,0:T(8,128)(2,1)} %q_hbm.1, bf16[128,512]{1,0:T(8,128)(2,1)} %k_hbm.1, bf16[128,512]{1,0:T(8,128)(2,1)} %v_hbm.1, f32[1,128]{1,0:T(1,128)} %bitcast.12, f32[1,128]{1,0:T(1,128)} %bitcast.13, bf16[1024,2048]{1,0:T(8,128)(2,1)} %wo_hbm.1, ...), custom_call_target="tpu_custom_call" | custom-call | tf_op jit(solution)/shard_map/fused/pallas_call | solution.py:704
  49.4 1.7 %hand_over.1 = (bf16[32,2048]{1,0:T(8,128)(2,1)}, bf16[128,512]{1,0:T(8,128)(2,1)}) custom-call(bf16[32,2048]{1,0:T(8,128)(2,1)} %get-tuple-element.4.a_ref, bf16[128,512]{1,0:T(8,128)(2,1)} %get-tuple-element.5.b_ref), custom_call_target="tpu_custom_call" | custom-call | tf_op jit(solution)/shard_map/hand_over/pallas_call | solution.py:766
where the time goes:
time: 51.7 us; the launch traced here: 51 us
  Pallas kernels  50.4 us (97%)
  between operations  0.64 us (1%)
    pallas_call x1, Pallas kernels, kernel_form(): pl.pallas_call(functools.partial(fused, dims), name='fused', out_shape=(j...  48.7 us
    pallas_call x1, Pallas kernels, kernel_form(): pl.pallas_call(hand_over, name='hand_over', out_shape=tuple((jax.ShapeDty...  1.68 us

commit v1 on v0

--- a/solution.py
+++ b/solution.py
@@ -621,9 +621,7 @@
     results = ret[...].astype(f32).reshape(rows, slab).astype(bf16)
     first = jnp.dot(c0, results, preferred_element_type=f32)
     second = jnp.dot(c1, results, preferred_element_type=f32)
-    eout_ref[...] = (w0 * first + w1 * second).astype(bf16)
-    e_store = pltpu.make_async_copy(eout_ref, eout_hbm, wsem.at[9])
-    e_store.start()
+    eout_hbm[...] = (w0 * first + w1 * second).astype(bf16)
 
     def m_store(c):
         at = slice(c * chunk, (c + 1) * chunk)
@@ -634,8 +632,7 @@
         for i in range(3):
             wait_in(mrecv.at[c, i], mr.at[c, i])
             summed = summed + mrecv[c, i].astype(f32)
-        mixed_ref[c] = summed.astype(bf16)
-        m_store(c).start()
+        mixed_hbm[:, c * chunk : (c + 1) * chunk] = summed.astype(bf16)
 
     for d in range(1, n_ep):
         z_copy(d).wait_send()
@@ -657,14 +654,15 @@
     for c in range(4):
         for i in range(3):
             m_copy(i, c).wait_send()
-    e_store.wait()
-    for c in range(4):
-        m_store(c).wait()
-
-
-def hand_over(a_ref, b_ref, a_out, b_out):
-    a_out[...] = a_ref[...]
-    b_out[...] = b_ref[...]
+
+
+def hand_over(a_ref, b_ref, a_out, b_out, sem):
+    one = pltpu.make_async_copy(a_ref, a_out, sem.at[0])
+    two = pltpu.make_async_copy(b_ref, b_out, sem.at[1])
+    one.start()
+    two.start()
+    one.wait()
+    two.wait()
 
 
 def kernel_form(
@@ -705,11 +703,11 @@
         functools.partial(fused, dims),
         name="fused",
         out_shape=(
-            jax.ShapeDtypeStruct((share, out_weight.shape[1]), bf16),
-            jax.ShapeDtypeStruct((tokens, slab), bf16),
+            pltpu.VMEM((share, out_weight.shape[1]), bf16),
+            pltpu.VMEM((tokens, slab), bf16),
         ),
         in_specs=[hbm, hbm, hbm, vmem, vmem, hbm, hbm, vmem, vmem, vmem, hbm, hbm, hbm, hbm],
-        out_specs=(hbm, hbm),
+        out_specs=(vmem, vmem),
         scratch_shapes=[
             pltpu.VMEM((4, share, out_weight.shape[1] // 4), bf16),
             pltpu.VMEM((tokens, slab), bf16),
@@ -763,13 +761,15 @@
         down_weight,
         table,
     )
+    vm = lambda o: pltpu.with_memory_space_constraint(o, pltpu.VMEM)
     return pl.pallas_call(
         hand_over,
         name="hand_over",
         out_shape=tuple(jax.ShapeDtypeStruct(o.shape, o.dtype) for o in outs),
         in_specs=[vmem, vmem],
-        out_specs=(vmem, vmem),
-    )(*outs)
+        out_specs=(hbm, hbm),
+        scratch_shapes=[dma((2,))],
+    )(*(vm(o) for o in outs))
 
 
 def dispatch_form(mesh, *args):

time: 51.7 us -> 50.3 us (0.973)
  Pallas kernels: 50.4 us -> 48.9 us
    pallas_call x1, Pallas kernels: 1.68 us -> 0.72 us  [kernel_form(): pl.pallas_call(hand_over, name='hand_over', out_shape=tuple((jax.ShapeDty...]
where the time goes in v1:
time: 50.3 us; the launch traced here: 49.6 us
  Pallas kernels  48.9 us (97%)
  between operations  0.64 us (1%)
    pallas_call x1, Pallas kernels, kernel_form(): pl.pallas_call(functools.partial(fused, dims), name='fused', out_shape=(p...  48.2 us

profile of v1, /device:TPU:0, one launch (start us, length us, event | category | flops | bytes accessed | tf_op | source)
XLA Modules:
  0.0 49.6 jit_solution(14885715065458762984)
XLA Ops:
  0.6 48.2 %fused.1 = (bf16[32,2048]{1,0:T(8,128)(2,1)S(1)}, bf16[128,512]{1,0:T(8,128)(2,1)S(1)}) custom-call(bf16[128,1024]{1,0:T(8,128)(2,1)} %q_hbm.1, bf16[128,512]{1,0:T(8,128)(2,1)} %k_hbm.1, bf16[128,512]{1,0:T(8,128)(2,1)} %v_hbm.1, f32[1,128]{1,0:T(1,128)} %bitcast.12, f32[1,128]{1,0:T(1,128)} %bitcast.13, bf16[1024,2048]{1,0:T(8,128)(2,1)} %wo_hbm.1, ...), custom_call_target="tpu_custom_call" | custom-call | tf_op jit(solution)/shard_map/fused/pallas_call | solution.py:702
  48.9 0.7 %hand_over.1 = (bf16[32,2048]{1,0:T(8,128)(2,1)}, bf16[128,512]{1,0:T(8,128)(2,1)}) custom-call(bf16[32,2048]{1,0:T(8,128)(2,1)S(1)} %get-tuple-element.4.a_ref, bf16[128,512]{1,0:T(8,128)(2,1)S(1)} %get-tuple-element.5.b_ref), custom_call_target="tpu_custom_call" | custom-call | tf_op jit(solution)/shard_map/hand_over/pallas_call | solution.py:765

commit v2 on v1

v2 whole, which is shorter than its diff:
```python
import functools
import jax
import jax.numpy as jnp
import numpy as np
from jax import lax
from jax.experimental import pallas as pl
from jax.experimental.pallas import tpu as pltpu
from jax.sharding import PartitionSpec as P

GRID_W = 64


def rope_tables(count, offset, head_dim):
    pos = offset + lax.iota(jnp.int32, count)
    grid_row = (pos // GRID_W).astype(jnp.float32)
    grid_col = (pos % GRID_W).astype(jnp.float32)
    quarter = head_dim // 4
    inverse = 10000.0 ** (-jnp.arange(quarter, dtype=jnp.float32) / quarter)
    angles = jnp.concatenate([grid_row[:, None] * inverse, grid_col[:, None] * inverse], axis=-1)
    return (jnp.cos(angles), jnp.sin(angles))


def norm_rotate(x, gain, cosine, sine):
    count, number, head_dim = x.shape
    y = x * lax.rsqrt(jnp.mean(x * x, axis=-1, keepdims=True) + 1e-06) * gain
    pairs = y.reshape(count, number, head_dim // 2, 2)
    first, second = (pairs[..., 0], pairs[..., 1])
    cos_b = cosine[:, None, :]
    sin_b = sine[:, None, :]
    turned = jnp.stack([first * cos_b - second * sin_b, first * sin_b + second * cos_b], axis=-1)
    return turned.reshape(count, number, head_dim).astype(jnp.bfloat16)


def key_block_size(length, shard_rows):
    if length <= 2048:
        return length
    shards = length // shard_rows
    most = max(1, 2048 // shard_rows)
    best = 1
    for count in range(1, most + 1):
        if shards % count == 0:
            best = count
    return best * shard_rows


def local(
    queries,
    keys,
    values,
    query_gain,
    key_gain,
    out_weight,
    expert_input,
    norm_gain,
    routes,
    route_logits,
    gate_weight,
    up_weight,
    down_weight,
):
    tokens_here = queries.shape[0]
    head_dim = query_gain.shape[0]
    heads_here = queries.shape[1] // head_dim
    kv_here = keys.shape[1] // head_dim
    group = heads_here // kv_here
    offset = lax.axis_index("ep") * tokens_here
    cosine, sine = rope_tables(tokens_here, offset, head_dim)
    q_rot = norm_rotate(
        queries.astype(jnp.float32).reshape(tokens_here, heads_here, head_dim),
        query_gain,
        cosine,
        sine,
    )
    k_rot = norm_rotate(
        keys.astype(jnp.float32).reshape(tokens_here, kv_here, head_dim), key_gain, cosine, sine
    ).reshape(tokens_here, kv_here * head_dim)
    q_grouped = q_rot.reshape(tokens_here, kv_here, group, head_dim).transpose(1, 2, 0, 3)
    q_grouped = q_grouped.reshape(kv_here, group * tokens_here, head_dim)
    query_rows = group * tokens_here
    scale = head_dim ** (-0.5)
    start_state = (
        jnp.full((kv_here, query_rows), -1e30, jnp.float32),
        jnp.zeros((kv_here, query_rows), jnp.float32),
        jnp.zeros((kv_here, query_rows, head_dim), jnp.float32),
    )
    key_piece = lax.all_gather(k_rot, "ep", axis=0, tiled=True)
    value_piece = lax.all_gather(values, "ep", axis=0, tiled=True)
    length = key_piece.shape[0]
    block = key_block_size(length, tokens_here)
    key_blocks = key_piece.reshape(length // block, block, kv_here, head_dim)
    value_blocks = value_piece.reshape(length // block, block, kv_here, head_dim)

    def step(state, blocks):
        running_max, running_total, running_sum = state
        key_block, value_block = blocks
        scores = (
            jnp.einsum("kqd,lkd->kql", q_grouped, key_block, preferred_element_type=jnp.float32)
            * scale
        )
        new_max = jnp.maximum(running_max, jnp.max(scores, axis=-1))
        factor = jnp.exp(running_max - new_max)
        weights = jnp.exp(scores - new_max[..., None])
        new_total = running_total * factor + jnp.sum(weights, axis=-1)
        new_sum = running_sum * factor[..., None] + jnp.einsum(
            "kql,lkd->kqd",
            weights.astype(jnp.bfloat16),
            value_block,
            preferred_element_type=jnp.float32,
        )
        return ((new_max, new_total, new_sum), None)

    result, _ = lax.scan(step, start_state, (key_blocks, value_blocks))
    final_max, final_total, final_sum = result
    attended = (final_sum / final_total[..., None]).astype(jnp.bfloat16)
    attended = attended.reshape(kv_here, group, tokens_here, head_dim).transpose(2, 0, 1, 3)
    attended = attended.reshape(tokens_here, heads_here * head_dim)
    summed = lax.psum_scatter(
        jnp.dot(attended, out_weight, preferred_element_type=jnp.float32).astype(jnp.bfloat16),
        "tp",
        scatter_dimension=0,
        tiled=True,
    ).astype(jnp.float32)
    mixed = summed.astype(jnp.bfloat16)
    expert_tokens_here, width = expert_input.shape
    n_ep = lax.axis_size("ep")
    top = routes.shape[1]
    capacity = expert_tokens_here * top // n_ep * 5 // 4
    x = expert_input.astype(jnp.float32)
    normed = (x * lax.rsqrt(jnp.mean(x * x, axis=-1, keepdims=True) + 1e-06) * norm_gain).astype(
        jnp.bfloat16
    )
    expert_ids = routes.reshape(-1)
    onehot = (expert_ids[:, None] == lax.iota(jnp.int32, n_ep)[None, :]).astype(jnp.int32)
    before = jnp.cumsum(onehot, axis=0) - onehot
    slot = jnp.sum(before * onehot, axis=1)
    target = expert_ids * capacity + slot
    owner_row = lax.iota(jnp.int32, expert_tokens_here * top) // top
    w_gate = gate_weight[0]
    w_up = up_weight[0]
    w_down = down_weight[0]
    columns = normed.shape[1]
    filled = jnp.zeros((n_ep * capacity, columns), jnp.bfloat16).at[target].set(normed[owner_row])
    arrived = lax.all_to_all(
        filled.reshape(n_ep, capacity, columns), "ep", split_axis=0, concat_axis=0, tiled=True
    )
    sources, slots, work_columns = arrived.shape
    flat = arrived.reshape(sources * slots, work_columns)
    gate = jnp.dot(flat, w_gate, preferred_element_type=jnp.float32)
    upper = jnp.dot(flat, w_up, preferred_element_type=jnp.float32)
    hidden = (jax.nn.silu(gate) * upper).astype(jnp.bfloat16)
    partial_out = jnp.dot(hidden, w_down, preferred_element_type=jnp.float32)
    summed = lax.psum_scatter(
        partial_out.reshape(sources, slots, width).astype(jnp.bfloat16),
        "tp",
        scatter_dimension=2,
        tiled=True,
    ).astype(jnp.float32)
    returned = lax.all_to_all(
        summed.astype(jnp.bfloat16), "ep", split_axis=0, concat_axis=0, tiled=True
    )
    picked = returned.reshape(n_ep * capacity, -1)[target].reshape(expert_tokens_here, top, -1)
    route_weight = jax.nn.sigmoid(route_logits - route_logits[:, ::-1])
    combined = jnp.sum(route_weight[..., None] * picked.astype(jnp.float32), axis=1)
    expert_out = combined.astype(jnp.bfloat16)
    return (mixed, expert_out)


MESH = pl.DeviceIdType.MESH


def rope_constants(length, head_dim):
    pos = np.arange(length)
    quarter = head_dim // 4
    inverse = (np.float32(10000.0) ** (-np.arange(quarter, dtype=np.float32) / np.float32(quarter))).astype(np.float32)
    grid_row = (pos // GRID_W).astype(np.float32)
    grid_col = (pos % GRID_W).astype(np.float32)
    angles = np.concatenate([grid_row[:, None] * inverse, grid_col[:, None] * inverse], axis=-1)
    cosine = np.repeat(np.cos(angles), 2, axis=-1).astype(np.float32)
    sine = np.repeat(np.sin(angles), 2, axis=-1).astype(np.float32)
    sine[:, 0::2] *= -1.0
    return np.stack([cosine, sine])


def fused(
    dims,
    q_hbm,
    k_hbm,
    v_hbm,
    qg_hbm,
    kg_hbm,
    wo_hbm,
    x_hbm,
    ng_hbm,
    rt_hbm,
    lg_hbm,
    wg_hbm,
    wu_hbm,
    wd_hbm,
    rope_hbm,
    mixed_ref,
    eout_ref,
    q_ref,
    k_ref,
    x_ref,
    qg_ref,
    kg_ref,
    ng_ref,
    rt_ref,
    lg_ref,
    wo,
    wg,
    wu,
    wd,
    rope,
    disp,
    xq,
    gacc,
    uacc,
    hid,
    part,
    rdiag,
    rs,
    back,
    ret,
    kv,
    qrot,
    qship,
    att,
    aship,
    macc,
    mpart,
    mrecv,
    wsem,
    ssem,
    zr,
    axr,
    ayr,
    afr,
    kvr,
    kvm,
    qsr,
    atr,
    rdr,
    rsr,
    br,
    mr,
):
    n_ep, cap, head_dim, kv_here, group = dims
    f32, bf16 = jnp.float32, jnp.bfloat16
    chips = n_ep // 2
    me = lax.axis_index("ep")
    t = lax.axis_index("tp")
    tx = t + 1 - 2 * (t % 2)
    ty = (t + 2) % 4
    td = 3 - t
    z = me // 2
    core = me % 2
    mate = 2 * z + 1 - core
    inner = (z == 1) | (z == 2)
    partner = z + 1 - 2 * (z % 2)
    other = 3 - z
    far_end = 3 - partner
    near = [partner, jnp.where(z < 2, 2, 1), jnp.where(z < 2, 3, 0)]
    order = [me, mate]
    for chip in near:
        order += [2 * chip + core, 2 * chip + 1 - core]
    far_first = order[::-1]
    first_to = []
    for chip in (partner, jnp.where(inner, other, far_end), jnp.where(inner, far_end, other)):
        first_to += [2 * chip + core, 2 * chip + 1 - core]
    tokens = x_ref.shape[0]
    slab = disp.shape[2]
    rows = n_ep * cap
    half = n_ep // 2

    loads = [
        (x_hbm, x_ref),
        (rt_hbm, rt_ref),
        (ng_hbm, ng_ref),
        (k_hbm, k_ref),
        (rope_hbm.at[:, pl.ds(pl.multiple_of(me * tokens, tokens), tokens), :], rope),
        (kg_hbm, kg_ref),
    ]
    for g in range(kv_here):
        loads.append((v_hbm.at[:, g * head_dim : (g + 1) * head_dim], kv.at[g, core, z, 1]))
    loads += [
        (q_hbm, q_ref),
        (qg_hbm, qg_ref),
        (lg_hbm, lg_ref),
        (wg_hbm.at[0], wg),
        (wu_hbm.at[0], wu),
        (wd_hbm.at[0], wd),
        (wo_hbm, wo),
    ]
    loads = [pltpu.make_async_copy(a, b, wsem.at[i]) for i, (a, b) in enumerate(loads)]
    x_load, rt_load, ng_load, k_load, rope_load, kg_load = loads[:6]
    v_loads = loads[6 : 6 + kv_here]
    q_load, qg_load, lg_load, wg_load, wu_load, wd_load, wo_load = loads[6 + kv_here :]
    x_load.start()
    rt_load.start()

    barrier = pltpu.get_barrier_semaphore()
    for d in range(1, n_ep):
        pl.semaphore_signal(barrier, inc=1, device_id={"ep": (me + d) % n_ep}, device_id_type=MESH)
    for peer in (tx, ty, td):
        pl.semaphore_signal(barrier, inc=1, device_id={"tp": peer}, device_id_type=MESH)
    for load in loads[2:]:
        load.start()

    rt_load.wait()
    wide = (tokens, tokens)
    lane = lax.broadcasted_iota(jnp.int32, wide, 1)
    sub = lax.broadcasted_iota(jnp.int32, wide, 0)
    routed = (sub == rt_ref[0:1, :]) | (sub == rt_ref[1:2, :])
    named_t = jnp.where(routed, 1.0, 0.0)
    upper = jnp.where(sub < lane, 1.0, 0.0).astype(bf16)
    rank_t = jnp.dot(named_t.astype(bf16), upper, preferred_element_type=f32)
    slot_iota = lax.broadcasted_iota(jnp.int32, (cap, tokens), 0).astype(f32)
    picks = [
        jnp.where((slot_iota == rank_t[e : e + 1, :]) & (named_t[e : e + 1, :] > 0.5), 1.0, 0.0)
        for e in range(n_ep)
    ]
    pick = jnp.concatenate(picks, axis=0).astype(bf16)

    ng_load.wait()
    x_load.wait()
    x = x_ref[...].astype(f32)
    inv = lax.rsqrt(jnp.mean(x * x, axis=-1, keepdims=True) + 1e-06)
    cols = pl.ds(pl.multiple_of(t * slab, slab), slab)
    normed = (x_ref[:, cols].astype(f32) * inv * ng_ref[:, cols]).astype(bf16)
    sent = jnp.dot(pick, normed, preferred_element_type=f32)
    for e in range(n_ep):
        disp[e] = sent[e * cap : (e + 1) * cap].astype(bf16)
    xq[t, me] = disp[me]

    pl.semaphore_wait(barrier, n_ep - 1 + 3)

    def remote(a, b, s, r, **where):
        return pltpu.make_async_remote_copy(
            src_ref=a, dst_ref=b, send_sem=s, recv_sem=r, device_id=where, device_id_type=MESH
        )

    def wait_in(ref, sem):
        remote(ref, ref, ssem.at[0], sem, tp=tx).wait_recv()

    def wait_out(ref, sem):
        remote(ref, ref, sem, zr.at[0], tp=tx).wait_send()

    for e in [mate] + first_to:
        remote(disp.at[e], xq.at[t, me], ssem.at[0], zr.at[me], ep=e).start()

    def spread(i):
        s = order[i]
        even = i % 2 == 0
        at_x, at_y = (i // 2, half) if even else (half, i // 2)
        remote(xq.at[t, s], xq.at[t, s], ssem.at[1], axr.at[at_x], tp=tx).start()
        remote(xq.at[t, s], xq.at[t, s], ssem.at[1], ayr.at[at_y], tp=ty).start()

    def forward(i):
        s = order[i]
        if i % 2 == 0:
            wait_in(xq.at[tx, s], axr.at[i // 2])
            remote(xq.at[tx, s], xq.at[tx, s], ssem.at[1], afr.at[0], tp=ty).start()
        else:
            wait_in(xq.at[ty, s], ayr.at[i // 2])
            remote(xq.at[ty, s], xq.at[ty, s], ssem.at[1], afr.at[0], tp=tx).start()

    spread(0)

    rope_load.wait()
    cos = rope[0]
    sin = rope[1]
    even = lax.broadcasted_iota(jnp.int32, (tokens, head_dim), 1) % 2 == 0

    def turn(piece, gain):
        a = piece.astype(f32)
        y = a * lax.rsqrt(jnp.mean(a * a, axis=-1, keepdims=True) + 1e-06) * gain
        other = jnp.where(even, pltpu.roll(y, head_dim - 1, 1), pltpu.roll(y, 1, 1))
        return (y * cos + other * sin).astype(bf16)

    kg_load.wait()
    k_load.wait()
    for g in range(kv_here):
        kv[g, core, z, 0] = turn(k_ref[:, g * head_dim : (g + 1) * head_dim], kg_ref[...])

    def kv_send(g, chip, to):
        block = kv.at[g, core, chip]
        remote(block, block, ssem.at[3], kvr.at[g, chip], ep=2 * to + core).start()

    def kv_mate(g, chip):
        block = kv.at[g, core, chip]
        remote(block, block, ssem.at[2], kvm.at[g], ep=mate).start()

    for v_load in v_loads:
        v_load.wait()

    def receive(i):
        wait_in(xq.at[t, order[i]], zr.at[order[i]])
        spread(i)

    receive(1)
    q_load.wait()
    qg_load.wait()
    for h in range(kv_here * group):
        qrot[h] = turn(q_ref[:, h * head_dim : (h + 1) * head_dim], qg_ref[...])
    q_of = lambda g: qrot.at[pl.ds(g * group, group)]

    lag = 4
    for i in range(2, n_ep):
        receive(i)
        if i == 3:

            @pl.when(~inner)
            def _():
                for g in range(kv_here):
                    kv_send(g, z, partner)
                    remote(q_of(g), qship.at[g], ssem.at[3], qsr.at[g], ep=2 * partner + core).start()

        if i >= lag:
            forward(i - lag)

    @pl.when(inner)
    def _():
        for g in range(kv_here):
            kv_send(g, z, other)
            kv_mate(g, z)

    def relay_kv(source, on):
        @pl.when(inner)
        def _():
            for g in range(kv_here):
                block = kv.at[g, core, source]
                wait_in(block, kvr.at[g, source])
                if on:
                    kv_send(g, source, other)
                kv_mate(g, source)

    wg_load.wait()
    wu_load.wait()

    def gate_up(q, first):
        block = xq[q].astype(f32).reshape(rows, slab).astype(bf16)
        at = pl.ds(pl.multiple_of(q * slab, slab), slab)
        g = lax.dot_general(block, wg[:, at], (((1,), (1,)), ((), ())), preferred_element_type=f32)
        u = lax.dot_general(block, wu[:, at], (((1,), (1,)), ((), ())), preferred_element_type=f32)
        if first:
            gacc[...] = g
            uacc[...] = u
        else:
            gacc[...] += g
            uacc[...] += u

    gate_up(t, True)
    for i in range(n_ep - lag, n_ep):
        forward(i)
    wait_in(xq.at[tx, pl.ds(0, half)], axr.at[half])
    wait_in(xq.at[ty, pl.ds(0, half)], ayr.at[half])
    gate_up(tx, False)
    gate_up(ty, False)
    relay_kv(partner, True)
    wait_in(xq.at[td], afr.at[0])
    gate_up(td, False)
    gate = gacc[...]
    hid[...] = (gate / (1.0 + jnp.exp(-gate)) * uacc[...]).astype(bf16)
    wd_load.wait()

    def down(q):
        at = pl.ds(pl.multiple_of(q * slab, slab), slab)
        out = jnp.dot(hid[...], wd[:, at], preferred_element_type=f32)
        for s in range(n_ep):
            part[q, s] = out[s * cap : (s + 1) * cap].astype(bf16)

    def rx_copy(s):
        remote(part.at[tx, s], rs.at[0, s], ssem.at[6], rsr.at[s], tp=tx).start()

    def ry_copy(s):
        remote(part.at[ty, s], rs.at[1, s], ssem.at[6], rsr.at[s], tp=ty).start()

    down(td)
    for i in range(n_ep):
        s = far_first[i]
        remote(part.at[td, s], rdiag.at[s], ssem.at[6], rdr.at[s], tp=tx if i % 2 == 0 else ty).start()
    down(tx)
    for i in range(0, n_ep, 2):
        rx_copy(far_first[i])
    down(ty)
    for i in range(1, n_ep, 2):
        ry_copy(far_first[i])
    down(t)
    relay_kv(other, False)
    relay_kv(far_end, False)
    scale = head_dim ** (-0.5) * 1.4426950408889634
    share = tokens // 4
    width = wo.shape[1]
    chunk = width // 4

    def attend_one(g, q2):
        keys = kv[g, :, :, 0].reshape(n_ep * tokens, head_dim)
        vals = kv[g, :, :, 1].reshape(n_ep * tokens, head_dim)
        q2 = q2.reshape(group * tokens, head_dim)
        s = lax.dot_general(q2, keys, (((1,), (1,)), ((), ())), preferred_element_type=f32)
        peak = jnp.max(s, axis=-1, keepdims=True)
        p = jnp.exp2((s - peak) * scale)
        total = jnp.sum(p, axis=-1, keepdims=True)
        out = jnp.dot(p.astype(bf16), vals, preferred_element_type=f32) / total
        return jnp.concatenate([out[r * tokens : (r + 1) * tokens] for r in range(group)], axis=1).astype(bf16)

    def attend(g):
        @pl.when(inner)
        def _():
            wait_in(qship.at[g], qsr.at[g])
            wait_in(kv.at[g, 1 - core], kvm.at[g])
            aship[g] = attend_one(g, qship[g])
            remote(aship.at[g], att.at[g], ssem.at[3], atr.at[g], ep=2 * partner + core).start()
            att[g] = attend_one(g, qrot[g * group : (g + 1) * group])

    def meet(i):
        s = far_first[i]
        wait_in(rdiag.at[s], rdr.at[s])
        if i % 2 == 0:
            part[ty, s] = (part[ty, s].astype(f32) + rdiag[s].astype(f32)).astype(bf16)
            ry_copy(s)
        else:
            part[tx, s] = (part[tx, s].astype(f32) + rdiag[s].astype(f32)).astype(bf16)
            rx_copy(s)

    def finish(i):
        s = far_first[i]
        wait_in(rs.at[0, pl.ds(0, 2)], rsr.at[s])
        out = (part[t, s].astype(f32) + rs[0, s].astype(f32) + rs[1, s].astype(f32)).astype(bf16)
        if i < n_ep - 1:
            back[s] = out
            remote(back.at[s], ret.at[me], ssem.at[7], br.at[0], ep=s).start()
        else:
            ret[s] = out

    attend(0)
    attend(1)
    for i in range(half):
        meet(i)
    attend(2)
    for i in range(half, n_ep):
        meet(i)
    attend(3)
    for i in range(n_ep):
        finish(i)

    @pl.when(~inner)
    def _():
        for g in range(kv_here):
            wait_in(att.at[g], atr.at[g])

    wo_load.wait()
    heads = jnp.concatenate([att[g] for g in range(kv_here)], axis=1)
    for c in range(4):
        at = slice(c * chunk, (c + 1) * chunk)
        out = jnp.dot(heads, wo[:, at], preferred_element_type=f32)
        for j in range(4):
            mpart[c, j] = out[j * share : (j + 1) * share].astype(bf16)
        for i, to in enumerate((td, tx, ty)):
            remote(mpart.at[c, to], mrecv.at[c, i], ssem.at[5], mr.at[c], tp=to).start()

    lg_load.wait()
    ids = rt_ref[...].astype(f32)
    logits = lg_ref[...]
    stacked = jnp.where(
        sub == 0,
        ids[0:1, :],
        jnp.where(sub == 1, ids[1:2, :], jnp.where(sub == 2, logits[0:1, :], logits[1:2, :])),
    )
    columns = stacked.T
    r0 = columns[:, 0:1].astype(jnp.int32)
    r1 = columns[:, 1:2].astype(jnp.int32)
    lower = jnp.where(lane < sub, 1.0, 0.0).astype(bf16)
    rank = jnp.dot(lower, named_t.T.astype(bf16), preferred_element_type=f32)
    total_lane = lax.broadcasted_iota(jnp.int32, (tokens, rows), 1)

    def chosen(r):
        slot = jnp.sum(jnp.where(lane == r, rank, 0.0), axis=-1, keepdims=True)
        target = r * cap + slot.astype(jnp.int32)
        return jnp.where(total_lane == target, 1.0, 0.0).astype(bf16)

    c0 = chosen(r0)
    c1 = chosen(r1)
    l0 = columns[:, 2:3]
    l1 = columns[:, 3:4]
    w0 = jax.nn.sigmoid(l0 - l1)
    w1 = jax.nn.sigmoid(l1 - l0)
    wait_in(ret.at[pl.ds(0, n_ep - 1)], br.at[0])
    results = ret[...].astype(f32).reshape(rows, slab).astype(bf16)
    first = jnp.dot(c0, results, preferred_element_type=f32)
    second = jnp.dot(c1, results, preferred_element_type=f32)
    eout_ref[...] = (w0 * first + w1 * second).astype(bf16)
    for c in range(4):
        wait_in(mrecv.at[c], mr.at[c])
        summed = mpart[c, t].astype(f32)
        for i in range(3):
            summed = summed + mrecv[c, i].astype(f32)
        mixed_ref[:, c * chunk : (c + 1) * chunk] = summed.astype(bf16)

    wait_out(disp.at[pl.ds(0, n_ep - 1)], ssem.at[0])
    wait_out(xq.at[pl.ds(0, 3)], ssem.at[1])

    @pl.when(inner)
    def _():
        wait_out(kv.at[:, 0], ssem.at[2])
        wait_out(kv.at[pl.ds(0, 3), 0], ssem.at[3])

    @pl.when(~inner)
    def _():
        wait_out(kv.at[pl.ds(0, 2), 0], ssem.at[3])

    wait_out(mrecv, ssem.at[5])
    wait_out(part.at[pl.ds(0, 3)], ssem.at[6])
    wait_out(back.at[pl.ds(0, n_ep - 1)], ssem.at[7])


def hand_over(a_ref, b_ref, a_out, b_out, sem):
    one = pltpu.make_async_copy(a_ref, a_out, sem.at[0])
    two = pltpu.make_async_copy(b_ref, b_out, sem.at[1])
    one.start()
    two.start()
    one.wait()
    two.wait()


def kernel_form(
    queries,
    keys,
    values,
    query_gain,
    key_gain,
    out_weight,
    expert_input,
    norm_gain,
    routes,
    route_logits,
    gate_weight,
    up_weight,
    down_weight,
):
    bf16, f32 = jnp.bfloat16, jnp.float32
    n_ep = lax.axis_size("ep")
    tokens = queries.shape[0]
    head_dim = query_gain.shape[0]
    heads = queries.shape[1] // head_dim
    kv_here = keys.shape[1] // head_dim
    width = expert_input.shape[1]
    n_tp = lax.axis_size("tp")
    slab = width // n_tp
    cap = tokens * routes.shape[1] // n_ep * 5 // 4
    rows = n_ep * cap
    ff = gate_weight.shape[2]
    share = tokens // n_tp
    chunk = out_weight.shape[1] // 4
    table = jnp.asarray(rope_constants(tokens * n_ep, head_dim))
    vmem = pl.BlockSpec(memory_space=pltpu.VMEM)
    hbm = pl.BlockSpec(memory_space=pl.ANY)
    piece = (n_ep, cap, slab)
    dma = pltpu.SemaphoreType.DMA
    dims = (n_ep, cap, head_dim, kv_here, heads // kv_here)
    outs = pl.pallas_call(
        functools.partial(fused, dims),
        name="fused",
        out_shape=(
            pltpu.VMEM((share, out_weight.shape[1]), bf16),
            pltpu.VMEM((tokens, slab), bf16),
        ),
        in_specs=[hbm] * 14,
        out_specs=(vmem, vmem),
        scratch_shapes=[
            pltpu.VMEM(queries.shape, bf16),
            pltpu.VMEM(keys.shape, bf16),
            pltpu.VMEM(expert_input.shape, bf16),
            pltpu.VMEM((1, head_dim), f32),
            pltpu.VMEM((1, head_dim), f32),
            pltpu.VMEM((1, width), f32),
            pltpu.VMEM((2, tokens), jnp.int32),
            pltpu.VMEM((2, tokens), f32),
            pltpu.VMEM(out_weight.shape, bf16),
            pltpu.VMEM((ff, width), bf16),
            pltpu.VMEM((ff, width), bf16),
            pltpu.VMEM(down_weight.shape[1:], bf16),
            pltpu.VMEM((2, tokens, head_dim), f32),
            pltpu.VMEM(piece, bf16),
            pltpu.VMEM((n_tp,) + piece, bf16),
            pltpu.VMEM((rows, ff), f32),
            pltpu.VMEM((rows, ff), f32),
            pltpu.VMEM((rows, ff), bf16),
            pltpu.VMEM((n_tp,) + piece, bf16),
            pltpu.VMEM(piece, bf16),
            pltpu.VMEM((2,) + piece, bf16),
            pltpu.VMEM(piece, bf16),
            pltpu.VMEM(piece, bf16),
            pltpu.VMEM((kv_here, 2, n_ep // 2, 2, tokens, head_dim), bf16),
            pltpu.VMEM((heads, tokens, head_dim), bf16),
            pltpu.VMEM((kv_here, heads // kv_here, tokens, head_dim), bf16),
            pltpu.VMEM((kv_here, tokens, heads // kv_here * head_dim), bf16),
            pltpu.VMEM((kv_here, tokens, heads // kv_here * head_dim), bf16),
            pltpu.VMEM((tokens, width), f32),
            pltpu.VMEM((4, n_tp, share, chunk), bf16),
            pltpu.VMEM((4, 3, share, chunk), bf16),
            dma((13 + kv_here,)),
            dma((8,)),
            dma((n_ep,)),
            dma((n_ep // 2 + 1,)),
            dma((n_ep // 2 + 1,)),
            dma((1,)),
            dma((kv_here, n_ep // 2)),
            dma((kv_here,)),
            dma((kv_here,)),
            dma((kv_here,)),
            dma((n_ep,)),
            dma((n_ep,)),
            dma((1,)),
            dma((4,)),
        ],
        compiler_params=pltpu.CompilerParams(
            collective_id=0, has_side_effects=True, vmem_limit_bytes=60 * 1024 * 1024
        ),
    )(
        queries,
        keys,
        values,
        query_gain.reshape(1, -1),
        key_gain.reshape(1, -1),
        out_weight,
        expert_input,
        norm_gain.reshape(1, -1),
        routes.T,
        route_logits.T,
        jnp.swapaxes(gate_weight, 1, 2),
        jnp.swapaxes(up_weight, 1, 2),
        down_weight,
        table,
    )
    return pl.pallas_call(
        hand_over,
        name="hand_over",
        out_shape=tuple(jax.ShapeDtypeStruct(o.shape, o.dtype) for o in outs),
        in_specs=[vmem, vmem],
        out_specs=(hbm, hbm),
        scratch_shapes=[dma((2,))],
    )(*(pltpu.with_memory_space_constraint(o, pltpu.VMEM) for o in outs))


def dispatch_form(mesh, *args):
    queries, routes = args[0], args[8]
    tokens = queries.shape[0]
    n_ep, n_tp = mesh.shape["ep"], mesh.shape["tp"]
    cap = tokens * routes.shape[1] // n_ep * 5 // 4
    same = args[6].shape[0] == tokens and tokens % 128 == 0
    fits = n_tp == 4 and n_ep == 8 and cap % 8 == 0
    if same and fits and routes.shape[1] == 2 and tokens == 128:
        return kernel_form(*args)
    return local(*args)


def solution(mesh):
    placed = (
        P("ep", "tp"),
        P("ep", "tp"),
        P("ep", "tp"),
        P(),
        P(),
        P("tp", None),
        P("ep", None),
        P(),
        P("ep", None),
        P("ep", None),
        P("ep", None, "tp"),
        P("ep", None, "tp"),
        P("ep", "tp", None),
    )
    return jax.shard_map(
        functools.partial(dispatch_form, mesh),
        mesh=mesh,
        in_specs=placed,
        out_specs=(P(("ep", "tp"), None), P("ep", "tp")),
        check_vma=False,
    )
```

time: 50.3 us -> 47.9 us (0.952); the launches traced: 49.6 us -> 47.7 us
  Pallas kernels: 48.9 us -> 47.1 us
    pallas_call x1, Pallas kernels: 48.2 us -> 46.4 us  [kernel_form(): pl.pallas_call(functools.partial(fused, dims), name='fused', out_shape=(p...]
where the time goes in v2:
time: 47.9 us; the launch traced here: 47.7 us
  Pallas kernels  47.1 us (98%)
  between operations  0.64 us (1%)
    pallas_call x1, Pallas kernels, kernel_form(): pl.pallas_call(functools.partial(fused, dims), name='fused', out_shape=(p...  46.4 us

profile of v2, /device:TPU:0, one launch (start us, length us, event | category | flops | bytes accessed | tf_op | source)
XLA Modules:
  0.0 47.7 jit_solution(4939966231614609731)
XLA Ops:
  0.6 46.4 %fused.1 = (bf16[32,2048]{1,0:T(8,128)(2,1)S(1)}, bf16[128,512]{1,0:T(8,128)(2,1)S(1)}) custom-call(bf16[128,1024]{1,0:T(8,128)(2,1)} %q_hbm.1, bf16[128,512]{1,0:T(8,128)(2,1)} %k_hbm.1, bf16[128,512]{1,0:T(8,128)(2,1)} %v_hbm.1, f32[1,128]{1,0:T(1,128)} %bitcast.12, f32[1,128]{1,0:T(1,128)} %bitcast.13, bf16[1024,2048]{1,0:T(8,128)(2,1)} %wo_hbm.1, ...), custom_call_target="tpu_custom_call" | custom-call | tf_op jit(solution)/shard_map/fused/pallas_call | solution.py:662
  47.0 0.7 %hand_over.1 = (bf16[32,2048]{1,0:T(8,128)(2,1)}, bf16[128,512]{1,0:T(8,128)(2,1)}) custom-call(bf16[32,2048]{1,0:T(8,128)(2,1)S(1)} %get-tuple-element.4.a_ref, bf16[128,512]{1,0:T(8,128)(2,1)S(1)} %get-tuple-element.5.b_ref), custom_call_target="tpu_custom_call" | custom-call | tf_op jit(solution)/shard_map/hand_over/pallas_call | solution.py:737

commit v3 on v2

--- a/solution.py
+++ b/solution.py
@@ -266,7 +266,7 @@
         order += [2 * chip + core, 2 * chip + 1 - core]
     far_first = order[::-1]
     first_to = []
-    for chip in (partner, jnp.where(inner, other, far_end), jnp.where(inner, far_end, other)):
+    for chip in (partner, other, far_end):
         first_to += [2 * chip + core, 2 * chip + 1 - core]
     tokens = x_ref.shape[0]
     slab = disp.shape[2]
@@ -405,19 +405,34 @@
         qrot[h] = turn(q_ref[:, h * head_dim : (h + 1) * head_dim], qg_ref[...])
     q_of = lambda g: qrot.at[pl.ds(g * group, group)]
 
-    lag = 4
-    for i in range(2, n_ep):
-        receive(i)
-        if i == 3:
-
-            @pl.when(~inner)
-            def _():
-                for g in range(kv_here):
-                    kv_send(g, z, partner)
-                    remote(q_of(g), qship.at[g], ssem.at[3], qsr.at[g], ep=2 * partner + core).start()
-
-        if i >= lag:
-            forward(i - lag)
+    receive(2)
+    receive(3)
+
+    @pl.when(~inner)
+    def _():
+        for g in range(kv_here):
+            kv_send(g, z, partner)
+        for g in range(kv_here):
+            remote(q_of(g), qship.at[g], ssem.at[3], qsr.at[g], ep=2 * partner + core).start()
+
+    forward(0)
+    forward(1)
+
+    @pl.when(~inner)
+    def _():
+        forward(2)
+        forward(3)
+
+    receive(4)
+    receive(5)
+
+    @pl.when(inner)
+    def _():
+        forward(2)
+        forward(3)
+
+    receive(6)
+    receive(7)
 
     @pl.when(inner)
     def _():
@@ -425,15 +440,18 @@
             kv_send(g, z, other)
             kv_mate(g, z)
 
-    def relay_kv(source, on):
+    def relay_kv(g, source, on):
+        block = kv.at[g, core, source]
+        wait_in(block, kvr.at[g, source])
+        if on:
+            kv_send(g, source, other)
+        kv_mate(g, source)
+
+    def relay_all(heads, source, on):
         @pl.when(inner)
         def _():
-            for g in range(kv_here):
-                block = kv.at[g, core, source]
-                wait_in(block, kvr.at[g, source])
-                if on:
-                    kv_send(g, source, other)
-                kv_mate(g, source)
+            for g in heads:
+                relay_kv(g, source, on)
 
     wg_load.wait()
     wu_load.wait()
@@ -451,13 +469,16 @@
             uacc[...] += u
 
     gate_up(t, True)
-    for i in range(n_ep - lag, n_ep):
-        forward(i)
+    forward(4)
+    forward(5)
+    relay_all((0, 1), partner, True)
+    forward(6)
+    forward(7)
     wait_in(xq.at[tx, pl.ds(0, half)], axr.at[half])
     wait_in(xq.at[ty, pl.ds(0, half)], ayr.at[half])
     gate_up(tx, False)
     gate_up(ty, False)
-    relay_kv(partner, True)
+    relay_all((2, 3), partner, True)
     wait_in(xq.at[td], afr.at[0])
     gate_up(td, False)
     gate = gacc[...]
@@ -487,8 +508,7 @@
     for i in range(1, n_ep, 2):
         ry_copy(far_first[i])
     down(t)
-    relay_kv(other, False)
-    relay_kv(far_end, False)
+    relay_all(range(kv_here), other, False)
     scale = head_dim ** (-0.5) * 1.4426950408889634
     share = tokens // 4
     width = wo.shape[1]
@@ -505,14 +525,12 @@
         out = jnp.dot(p.astype(bf16), vals, preferred_element_type=f32) / total
         return jnp.concatenate([out[r * tokens : (r + 1) * tokens] for r in range(group)], axis=1).astype(bf16)
 
-    def attend(g):
-        @pl.when(inner)
-        def _():
-            wait_in(qship.at[g], qsr.at[g])
-            wait_in(kv.at[g, 1 - core], kvm.at[g])
-            aship[g] = attend_one(g, qship[g])
-            remote(aship.at[g], att.at[g], ssem.at[3], atr.at[g], ep=2 * partner + core).start()
-            att[g] = attend_one(g, qrot[g * group : (g + 1) * group])
+    def attend_ship(g):
+        relay_kv(g, far_end, False)
+        wait_in(qship.at[g], qsr.at[g])
+        wait_in(kv.at[g, 1 - core], kvm.at[g])
+        aship[g] = attend_one(g, qship[g])
+        remote(aship.at[g], att.at[g], ssem.at[3], atr.at[g], ep=2 * partner + core).start()
 
     def meet(i):
         s = far_first[i]
@@ -534,16 +552,19 @@
         else:
             ret[s] = out
 
-    attend(0)
-    attend(1)
-    for i in range(half):
+
+    @pl.when(inner)
+    def _():
+        for g in range(kv_here):
+            attend_ship(g)
+
+    for i in range(n_ep):
         meet(i)
-    attend(2)
-    for i in range(half, n_ep):
-        meet(i)
-    attend(3)
-    for i in range(n_ep):
-        finish(i)
+
+    @pl.when(inner)
+    def _():
+        for g in range(kv_here):
+            att[g] = attend_one(g, qrot[g * group : (g + 1) * group])
 
     @pl.when(~inner)
     def _():
@@ -560,6 +581,8 @@
         for i, to in enumerate((td, tx, ty)):
             remote(mpart.at[c, to], mrecv.at[c, i], ssem.at[5], mr.at[c], tp=to).start()
 
+    for i in range(n_ep):
+        finish(i)
     lg_load.wait()
     ids = rt_ref[...].astype(f32)
     logits = lg_ref[...]

time: 47.9 us -> 45.1 us (0.942)
  Pallas kernels: 47.1 us -> 44.3 us
    pallas_call x1, Pallas kernels: 46.4 us -> 43.6 us  [kernel_form(): pl.pallas_call(functools.partial(fused, dims), name='fused', out_shape=(p...]
where the time goes in v3:
time: 45.1 us; the launch traced here: 45 us
  Pallas kernels  44.3 us (98%)
  between operations  0.64 us (1%)
    pallas_call x1, Pallas kernels, kernel_form(): pl.pallas_call(functools.partial(fused, dims), name='fused', out_shape=(p...  43.6 us

profile of v3, /device:TPU:0, one launch (start us, length us, event | category | flops | bytes accessed | tf_op | source)
XLA Modules:
  0.0 45.0 jit_solution(5632338705662301218)
XLA Ops:
  0.6 43.6 %fused.1 = (bf16[32,2048]{1,0:T(8,128)(2,1)S(1)}, bf16[128,512]{1,0:T(8,128)(2,1)S(1)}) custom-call(bf16[128,1024]{1,0:T(8,128)(2,1)} %q_hbm.1, bf16[128,512]{1,0:T(8,128)(2,1)} %k_hbm.1, bf16[128,512]{1,0:T(8,128)(2,1)} %v_hbm.1, f32[1,128]{1,0:T(1,128)} %bitcast.12, f32[1,128]{1,0:T(1,128)} %bitcast.13, bf16[1024,2048]{1,0:T(8,128)(2,1)} %wo_hbm.1, ...), custom_call_target="tpu_custom_call" | custom-call | tf_op jit(solution)/shard_map/fused/pallas_call | solution.py:685
  44.3 0.7 %hand_over.1 = (bf16[32,2048]{1,0:T(8,128)(2,1)}, bf16[128,512]{1,0:T(8,128)(2,1)}) custom-call(bf16[32,2048]{1,0:T(8,128)(2,1)S(1)} %get-tuple-element.4.a_ref, bf16[128,512]{1,0:T(8,128)(2,1)S(1)} %get-tuple-element.5.b_ref), custom_call_target="tpu_custom_call" | custom-call | tf_op jit(solution)/shard_map/hand_over/pallas_call | solution.py:760

commit v4 on v3

--- a/solution.py
+++ b/solution.py
@@ -261,17 +261,18 @@
     other = 3 - z
     far_end = 3 - partner
     near = [partner, jnp.where(z < 2, 2, 1), jnp.where(z < 2, 3, 0)]
+    half = n_ep // 2
     order = [me, mate]
     for chip in near:
         order += [2 * chip + core, 2 * chip + 1 - core]
-    far_first = order[::-1]
+    base = [half * (z // 2), half * (1 - z // 2)]
+    turns = [order[:half][::-1], order[half:][::-1]]
     first_to = []
     for chip in (partner, other, far_end):
         first_to += [2 * chip + core, 2 * chip + 1 - core]
     tokens = x_ref.shape[0]
     slab = disp.shape[2]
     rows = n_ep * cap
-    half = n_ep // 2
 
     loads = [
         (x_hbm, x_ref),
@@ -351,8 +352,8 @@
 
     def spread(i):
         s = order[i]
-        even = i % 2 == 0
-        at_x, at_y = (i // 2, half) if even else (half, i // 2)
+        rest = half + i // half
+        at_x, at_y = (i // 2, rest) if i % 2 == 0 else (rest, i // 2)
         remote(xq.at[t, s], xq.at[t, s], ssem.at[1], axr.at[at_x], tp=tx).start()
         remote(xq.at[t, s], xq.at[t, s], ssem.at[1], ayr.at[at_y], tp=ty).start()
 
@@ -360,10 +361,10 @@
         s = order[i]
         if i % 2 == 0:
             wait_in(xq.at[tx, s], axr.at[i // 2])
-            remote(xq.at[tx, s], xq.at[tx, s], ssem.at[1], afr.at[0], tp=ty).start()
+            remote(xq.at[tx, s], xq.at[tx, s], ssem.at[1], afr.at[i // half], tp=ty).start()
         else:
             wait_in(xq.at[ty, s], ayr.at[i // 2])
-            remote(xq.at[ty, s], xq.at[ty, s], ssem.at[1], afr.at[0], tp=tx).start()
+            remote(xq.at[ty, s], xq.at[ty, s], ssem.at[1], afr.at[i // half], tp=tx).start()
 
     spread(0)
 
@@ -405,6 +406,62 @@
         qrot[h] = turn(q_ref[:, h * head_dim : (h + 1) * head_dim], qg_ref[...])
     q_of = lambda g: qrot.at[pl.ds(g * group, group)]
 
+    def gate_up(q, k, first=False):
+        block = xq[q, pl.ds(base[k], half)].astype(f32).reshape(half * cap, slab).astype(bf16)
+        at = pl.ds(pl.multiple_of(q * slab, slab), slab)
+        g = lax.dot_general(block, wg[:, at], (((1,), (1,)), ((), ())), preferred_element_type=f32)
+        u = lax.dot_general(block, wu[:, at], (((1,), (1,)), ((), ())), preferred_element_type=f32)
+        if first:
+            gacc[k] = g
+            uacc[k] = u
+        else:
+            gacc[k] += g
+            uacc[k] += u
+
+    def sides(k):
+        wait_in(xq.at[tx, pl.ds(0, half // 2)], axr.at[half + k])
+        wait_in(xq.at[ty, pl.ds(0, half // 2)], ayr.at[half + k])
+
+    def corner(k):
+        wait_in(xq.at[td, pl.ds(0, half)], afr.at[k])
+
+    def activate(k):
+        gate = gacc[k]
+        hid[k] = (gate / (1.0 + jnp.exp(-gate)) * uacc[k]).astype(bf16)
+
+    def down(q, k):
+        at = pl.ds(pl.multiple_of(q * slab, slab), slab)
+        out = jnp.dot(hid[k], wd[:, at], preferred_element_type=f32)
+        for s in range(half):
+            part[q, base[k] + s] = out[s * cap : (s + 1) * cap].astype(bf16)
+
+    def rx_copy(s):
+        remote(part.at[tx, s], rs.at[0, s], ssem.at[6], rsr.at[s], tp=tx).start()
+
+    def ry_copy(s):
+        remote(part.at[ty, s], rs.at[1, s], ssem.at[6], rsr.at[s], tp=ty).start()
+
+    def send_far(k):
+        for j, s in enumerate(turns[k]):
+            remote(part.at[td, s], rdiag.at[s], ssem.at[6], rdr.at[s], tp=tx if j % 2 == 0 else ty).start()
+
+    def send_near(k):
+        for s in turns[k][0::2]:
+            rx_copy(s)
+        for s in turns[k][1::2]:
+            ry_copy(s)
+
+    def corner_far(k):
+        corner(k)
+        gate_up(td, k)
+        activate(k)
+        down(td, k)
+
+    def down_rest(k):
+        down(tx, k)
+        down(ty, k)
+        down(t, k)
+
     receive(2)
     receive(3)
 
@@ -418,97 +475,47 @@
     forward(0)
     forward(1)
 
+    wg_load.wait()
+    wu_load.wait()
+
     @pl.when(~inner)
     def _():
         forward(2)
         forward(3)
+        gate_up(t, 0, True)
 
     receive(4)
     receive(5)
 
     @pl.when(inner)
     def _():
+        kv_send(0, z, other)
+        kv_mate(0, z)
+        gate_up(t, 0, True)
         forward(2)
         forward(3)
 
     receive(6)
     receive(7)
 
-    @pl.when(inner)
-    def _():
-        for g in range(kv_here):
-            kv_send(g, z, other)
-            kv_mate(g, z)
-
-    def relay_kv(g, source, on):
-        block = kv.at[g, core, source]
-        wait_in(block, kvr.at[g, source])
-        if on:
-            kv_send(g, source, other)
-        kv_mate(g, source)
-
-    def relay_all(heads, source, on):
+    def own_kv(heads):
         @pl.when(inner)
         def _():
             for g in heads:
-                relay_kv(g, source, on)
-
-    wg_load.wait()
-    wu_load.wait()
-
-    def gate_up(q, first):
-        block = xq[q].astype(f32).reshape(rows, slab).astype(bf16)
-        at = pl.ds(pl.multiple_of(q * slab, slab), slab)
-        g = lax.dot_general(block, wg[:, at], (((1,), (1,)), ((), ())), preferred_element_type=f32)
-        u = lax.dot_general(block, wu[:, at], (((1,), (1,)), ((), ())), preferred_element_type=f32)
-        if first:
-            gacc[...] = g
-            uacc[...] = u
-        else:
-            gacc[...] += g
-            uacc[...] += u
-
-    gate_up(t, True)
-    forward(4)
-    forward(5)
-    relay_all((0, 1), partner, True)
-    forward(6)
-    forward(7)
-    wait_in(xq.at[tx, pl.ds(0, half)], axr.at[half])
-    wait_in(xq.at[ty, pl.ds(0, half)], ayr.at[half])
-    gate_up(tx, False)
-    gate_up(ty, False)
-    relay_all((2, 3), partner, True)
-    wait_in(xq.at[td], afr.at[0])
-    gate_up(td, False)
-    gate = gacc[...]
-    hid[...] = (gate / (1.0 + jnp.exp(-gate)) * uacc[...]).astype(bf16)
-    wd_load.wait()
-
-    def down(q):
-        at = pl.ds(pl.multiple_of(q * slab, slab), slab)
-        out = jnp.dot(hid[...], wd[:, at], preferred_element_type=f32)
-        for s in range(n_ep):
-            part[q, s] = out[s * cap : (s + 1) * cap].astype(bf16)
-
-    def rx_copy(s):
-        remote(part.at[tx, s], rs.at[0, s], ssem.at[6], rsr.at[s], tp=tx).start()
-
-    def ry_copy(s):
-        remote(part.at[ty, s], rs.at[1, s], ssem.at[6], rsr.at[s], tp=ty).start()
-
-    down(td)
-    for i in range(n_ep):
-        s = far_first[i]
-        remote(part.at[td, s], rdiag.at[s], ssem.at[6], rdr.at[s], tp=tx if i % 2 == 0 else ty).start()
-    down(tx)
-    for i in range(0, n_ep, 2):
-        rx_copy(far_first[i])
-    down(ty)
-    for i in range(1, n_ep, 2):
-        ry_copy(far_first[i])
-    down(t)
-    relay_all(range(kv_here), other, False)
+                kv_send(g, z, other)
+                kv_mate(g, z)
+
+    def relay_kv(heads, source, on):
+        @pl.when(inner)
+        def _():
+            for g in heads:
+                block = kv.at[g, core, source]
+                wait_in(block, kvr.at[g, source])
+                if on:
+                    kv_send(g, source, other)
+                kv_mate(g, source)
+
+    own_kv((1,))
     scale = head_dim ** (-0.5) * 1.4426950408889634
     share = tokens // 4
     width = wo.shape[1]
@@ -525,64 +532,120 @@
         out = jnp.dot(p.astype(bf16), vals, preferred_element_type=f32) / total
         return jnp.concatenate([out[r * tokens : (r + 1) * tokens] for r in range(group)], axis=1).astype(bf16)
 
-    def attend_ship(g):
-        relay_kv(g, far_end, False)
-        wait_in(qship.at[g], qsr.at[g])
-        wait_in(kv.at[g, 1 - core], kvm.at[g])
-        aship[g] = attend_one(g, qship[g])
-        remote(aship.at[g], att.at[g], ssem.at[3], atr.at[g], ep=2 * partner + core).start()
-
-    def meet(i):
-        s = far_first[i]
-        wait_in(rdiag.at[s], rdr.at[s])
-        if i % 2 == 0:
-            part[ty, s] = (part[ty, s].astype(f32) + rdiag[s].astype(f32)).astype(bf16)
-            ry_copy(s)
-        else:
-            part[tx, s] = (part[tx, s].astype(f32) + rdiag[s].astype(f32)).astype(bf16)
-            rx_copy(s)
-
-    def finish(i):
-        s = far_first[i]
-        wait_in(rs.at[0, pl.ds(0, 2)], rsr.at[s])
-        out = (part[t, s].astype(f32) + rs[0, s].astype(f32) + rs[1, s].astype(f32)).astype(bf16)
-        if i < n_ep - 1:
-            back[s] = out
-            remote(back.at[s], ret.at[me], ssem.at[7], br.at[0], ep=s).start()
-        else:
-            ret[s] = out
-
+    def attend_ship(heads):
+        @pl.when(inner)
+        def _():
+            for g in heads:
+                wait_in(qship.at[g], qsr.at[g])
+                wait_in(kv.at[g, 1 - core], kvm.at[g])
+                aship[g] = attend_one(g, qship[g])
+                remote(aship.at[g], att.at[g], ssem.at[3], atr.at[g], ep=2 * partner + core).start()
+
+    def meet(k):
+        for j, s in enumerate(turns[k]):
+            wait_in(rdiag.at[s], rdr.at[s])
+            if j % 2 == 0:
+                part[ty, s] = (part[ty, s].astype(f32) + rdiag[s].astype(f32)).astype(bf16)
+                ry_copy(s)
+            else:
+                part[tx, s] = (part[tx, s].astype(f32) + rdiag[s].astype(f32)).astype(bf16)
+                rx_copy(s)
+
+    def finish(k):
+        for j, s in enumerate(turns[k]):
+            wait_in(rs.at[0, pl.ds(0, 2)], rsr.at[s])
+            out = (part[t, s].astype(f32) + rs[0, s].astype(f32) + rs[1, s].astype(f32)).astype(bf16)
+            if k == 0 and j == half - 1:
+                ret[s] = out
+            else:
+                back[s] = out
+                remote(back.at[s], ret.at[me], ssem.at[7], br.at[0], ep=s).start()
+
+    share = tokens // 4
+    width = wo.shape[1]
+    chunk = width // 4
+
+    wd_load.wait()
+    sides(0)
+    gate_up(tx, 0)
+    gate_up(ty, 0)
+
+    @pl.when(~inner)
+    def _():
+        corner_far(0)
+        down_rest(0)
+
+    forward(4)
+    forward(5)
+    relay_kv((0,), partner, True)
+    own_kv((2,))
 
     @pl.when(inner)
     def _():
-        for g in range(kv_here):
-            attend_ship(g)
-
-    for i in range(n_ep):
-        meet(i)
+        corner_far(0)
+
+    send_far(0)
+    forward(6)
+    forward(7)
+    relay_kv((1,), partner, True)
+    own_kv((3,))
+    relay_kv((0, 1), other, False)
+
+    @pl.when(inner)
+    def _():
+        down_rest(0)
+
+    send_near(0)
+    relay_kv((2, 3), partner, True)
+    relay_kv((0,), far_end, False)
+    gate_up(t, 1, True)
+    sides(1)
+    gate_up(tx, 1)
+    gate_up(ty, 1)
+    attend_ship((0,))
+    relay_kv((2,), other, False)
+    relay_kv((1,), far_end, False)
+    corner_far(1)
+    send_far(1)
+    down_rest(1)
+    send_near(1)
+    meet(0)
+    attend_ship((1,))
+    relay_kv((3,), other, False)
+    relay_kv((2,), far_end, False)
+    relay_kv((3,), far_end, False)
+    attend_ship((2, 3))
+    meet(1)
 
     @pl.when(inner)
     def _():
         for g in range(kv_here):
             att[g] = attend_one(g, qrot[g * group : (g + 1) * group])
 
-    @pl.when(~inner)
-    def _():
-        for g in range(kv_here):
-            wait_in(att.at[g], atr.at[g])
-
+    finish(0)
+    finish(1)
+
+
+    def attended(heads):
+        @pl.when(~inner)
+        def _():
+            for g in heads:
+                wait_in(att.at[g], atr.at[g])
+
+    attended(range(kv_here - 1))
     wo_load.wait()
-    heads = jnp.concatenate([att[g] for g in range(kv_here)], axis=1)
+    cut = (kv_here - 1) * group * head_dim
+    early = jnp.concatenate([att[g] for g in range(kv_here - 1)], axis=1)
+    macc[...] = jnp.dot(early, wo[:cut, :], preferred_element_type=f32)
+    attended((kv_here - 1,))
     for c in range(4):
         at = slice(c * chunk, (c + 1) * chunk)
-        out = jnp.dot(heads, wo[:, at], preferred_element_type=f32)
+        out = macc[:, at] + jnp.dot(att[kv_here - 1], wo[cut:, at], preferred_element_type=f32)
         for j in range(4):
             mpart[c, j] = out[j * share : (j + 1) * share].astype(bf16)
         for i, to in enumerate((td, tx, ty)):
             remote(mpart.at[c, to], mrecv.at[c, i], ssem.at[5], mr.at[c], tp=to).start()
 
-    for i in range(n_ep):
-        finish(i)
     lg_load.wait()
     ids = rt_ref[...].astype(f32)
     logits = lg_ref[...]
@@ -707,9 +770,9 @@
             pltpu.VMEM((2, tokens, head_dim), f32),
             pltpu.VMEM(piece, bf16),
             pltpu.VMEM((n_tp,) + piece, bf16),
-            pltpu.VMEM((rows, ff), f32),
-            pltpu.VMEM((rows, ff), f32),
-            pltpu.VMEM((rows, ff), bf16),
+            pltpu.VMEM((2, rows // 2, ff), f32),
+            pltpu.VMEM((2, rows // 2, ff), f32),
+            pltpu.VMEM((2, rows // 2, ff), bf16),
             pltpu.VMEM((n_tp,) + piece, bf16),
             pltpu.VMEM(piece, bf16),
             pltpu.VMEM((2,) + piece, bf16),
@@ -726,9 +789,9 @@
             dma((13 + kv_here,)),
             dma((8,)),
             dma((n_ep,)),
-            dma((n_ep // 2 + 1,)),
-            dma((n_ep // 2 + 1,)),
-            dma((1,)),
+            dma((n_ep // 2 + 2,)),
+            dma((n_ep // 2 + 2,)),
+            dma((2,)),
             dma((kv_here, n_ep // 2)),
             dma((kv_here,)),
             dma((kv_here,)),

time: 45.1 us -> 42.3 us (0.938)
  Pallas kernels: 44.3 us -> 41.5 us
    pallas_call x1, Pallas kernels: 43.6 us -> 40.8 us  [kernel_form(): pl.pallas_call(functools.partial(fused, dims), name='fused', out_shape=(p...]
where the time goes in v4:
time: 42.3 us; the launch traced here: 42.1 us
  Pallas kernels  41.5 us (98%)
  between operations  0.64 us (2%)
    pallas_call x1, Pallas kernels, kernel_form(): pl.pallas_call(functools.partial(fused, dims), name='fused', out_shape=(p...  40.8 us

profile of v4, /device:TPU:0, one launch (start us, length us, event | category | flops | bytes accessed | tf_op | source)
XLA Modules:
  0.0 42.1 jit_solution(3529982095064661777)
XLA Ops:
  0.6 40.8 %fused.1 = (bf16[32,2048]{1,0:T(8,128)(2,1)S(1)}, bf16[128,512]{1,0:T(8,128)(2,1)S(1)}) custom-call(bf16[128,1024]{1,0:T(8,128)(2,1)} %q_hbm.1, bf16[128,512]{1,0:T(8,128)(2,1)} %k_hbm.1, bf16[128,512]{1,0:T(8,128)(2,1)} %v_hbm.1, f32[1,128]{1,0:T(1,128)} %bitcast.12, f32[1,128]{1,0:T(1,128)} %bitcast.13, bf16[1024,2048]{1,0:T(8,128)(2,1)} %wo_hbm.1, ...), custom_call_target="tpu_custom_call" | custom-call | tf_op jit(solution)/shard_map/fused/pallas_call | solution.py:748
  41.4 0.7 %hand_over.1 = (bf16[32,2048]{1,0:T(8,128)(2,1)}, bf16[128,512]{1,0:T(8,128)(2,1)}) custom-call(bf16[32,2048]{1,0:T(8,128)(2,1)S(1)} %get-tuple-element.4.a_ref, bf16[128,512]{1,0:T(8,128)(2,1)S(1)} %get-tuple-element.5.b_ref), custom_call_target="tpu_custom_call" | custom-call | tf_op jit(solution)/shard_map/hand_over/pallas_call | solution.py:823

commit v5 on v4

--- a/solution.py
+++ b/solution.py
@@ -202,14 +202,11 @@
     q_ref,
     k_ref,
     x_ref,
-    qg_ref,
-    kg_ref,
-    ng_ref,
+    gains,
     rt_ref,
     lg_ref,
     wo,
-    wg,
-    wu,
+    wgu,
     wd,
     rope,
     disp,
@@ -238,8 +235,7 @@
     afr,
     kvr,
     kvm,
-    qsr,
-    atr,
+    qar,
     rdr,
     rsr,
     br,
@@ -260,12 +256,12 @@
     partner = z + 1 - 2 * (z % 2)
     other = 3 - z
     far_end = 3 - partner
-    near = [partner, jnp.where(z < 2, 2, 1), jnp.where(z < 2, 3, 0)]
+    near = [jnp.where(inner, a, b) for a, b in ((other, partner), (partner, far_end), (far_end, other))]
     half = n_ep // 2
     order = [me, mate]
     for chip in near:
         order += [2 * chip + core, 2 * chip + 1 - core]
-    base = [half * (z // 2), half * (1 - z // 2)]
+    sides_of = [(z, near[0]), (near[1], near[2])]
     turns = [order[:half][::-1], order[half:][::-1]]
     first_to = []
     for chip in (partner, other, far_end):
@@ -274,41 +270,39 @@
     slab = disp.shape[2]
     rows = n_ep * cap
 
-    loads = [
-        (x_hbm, x_ref),
-        (rt_hbm, rt_ref),
-        (ng_hbm, ng_ref),
-        (k_hbm, k_ref),
-        (rope_hbm.at[:, pl.ds(pl.multiple_of(me * tokens, tokens), tokens), :], rope),
-        (kg_hbm, kg_ref),
-    ]
-    for g in range(kv_here):
-        loads.append((v_hbm.at[:, g * head_dim : (g + 1) * head_dim], kv.at[g, core, z, 1]))
-    loads += [
-        (q_hbm, q_ref),
-        (qg_hbm, qg_ref),
-        (lg_hbm, lg_ref),
-        (wg_hbm.at[0], wg),
-        (wu_hbm.at[0], wu),
-        (wd_hbm.at[0], wd),
-        (wo_hbm, wo),
-    ]
-    loads = [pltpu.make_async_copy(a, b, wsem.at[i]) for i, (a, b) in enumerate(loads)]
-    x_load, rt_load, ng_load, k_load, rope_load, kg_load = loads[:6]
-    v_loads = loads[6 : 6 + kv_here]
-    q_load, qg_load, lg_load, wg_load, wu_load, wd_load, wo_load = loads[6 + kv_here :]
-    x_load.start()
-    rt_load.start()
+    width = x_ref.shape[1]
+    ends = (0, width, width + head_dim, width + 2 * head_dim)
+    ng_ref, kg_ref, qg_ref = [gains.at[:, ends[i] : ends[i + 1]] for i in range(3)]
+
+    def load(i, a, b):
+        return pltpu.make_async_copy(a, b, wsem.at[i])
+
+    def loaded(i, ref):
+        load(i, ref, ref).wait()
+
+    load(0, x_hbm, x_ref).start()
+    load(1, rt_hbm, rt_ref).start()
 
     barrier = pltpu.get_barrier_semaphore()
     for d in range(1, n_ep):
         pl.semaphore_signal(barrier, inc=1, device_id={"ep": (me + d) % n_ep}, device_id_type=MESH)
     for peer in (tx, ty, td):
         pl.semaphore_signal(barrier, inc=1, device_id={"tp": peer}, device_id_type=MESH)
-    for load in loads[2:]:
-        load.start()
-
-    rt_load.wait()
+    load(2, ng_hbm, ng_ref).start()
+    load(2, kg_hbm, kg_ref).start()
+    load(2, qg_hbm, qg_ref).start()
+    load(3, k_hbm, k_ref).start()
+    load(4, rope_hbm.at[:, pl.ds(pl.multiple_of(me * tokens, tokens), tokens), :], rope).start()
+    for g in range(kv_here):
+        load(5, v_hbm.at[:, g * head_dim : (g + 1) * head_dim], kv.at[g, core, z, 1]).start()
+    load(6, q_hbm, q_ref).start()
+    load(7, lg_hbm, lg_ref).start()
+    load(8, wg_hbm.at[0], wgu.at[0]).start()
+    load(8, wu_hbm.at[0], wgu.at[1]).start()
+    load(9, wd_hbm.at[0], wd).start()
+    load(10, wo_hbm, wo).start()
+
+    loaded(1, rt_ref)
     wide = (tokens, tokens)
     lane = lax.broadcasted_iota(jnp.int32, wide, 1)
     sub = lax.broadcasted_iota(jnp.int32, wide, 0)
@@ -323,8 +317,8 @@
     ]
     pick = jnp.concatenate(picks, axis=0).astype(bf16)
 
-    ng_load.wait()
-    x_load.wait()
+    loaded(2, gains)
+    loaded(0, x_ref)
     x = x_ref[...].astype(f32)
     inv = lax.rsqrt(jnp.mean(x * x, axis=-1, keepdims=True) + 1e-06)
     cols = pl.ds(pl.multiple_of(t * slab, slab), slab)
@@ -347,8 +341,8 @@
     def wait_out(ref, sem):
         remote(ref, ref, sem, zr.at[0], tp=tx).wait_send()
 
-    for e in [mate] + first_to:
-        remote(disp.at[e], xq.at[t, me], ssem.at[0], zr.at[me], ep=e).start()
+    for e, i in zip([mate] + first_to, range(n_ep - 1)):
+        remote(disp.at[e], xq.at[t, me], ssem.at[0], zr.at[i], ep=e).start()
 
     def spread(i):
         s = order[i]
@@ -368,7 +362,7 @@
 
     spread(0)
 
-    rope_load.wait()
+    loaded(4, rope)
     cos = rope[0]
     sin = rope[1]
     even = lax.broadcasted_iota(jnp.int32, (tokens, head_dim), 1) % 2 == 0
@@ -379,38 +373,40 @@
         other = jnp.where(even, pltpu.roll(y, head_dim - 1, 1), pltpu.roll(y, 1, 1))
         return (y * cos + other * sin).astype(bf16)
 
-    kg_load.wait()
-    k_load.wait()
+    loaded(3, k_ref)
     for g in range(kv_here):
         kv[g, core, z, 0] = turn(k_ref[:, g * head_dim : (g + 1) * head_dim], kg_ref[...])
 
-    def kv_send(g, chip, to):
+    def kv_send(g, chip, to, kind):
         block = kv.at[g, core, chip]
-        remote(block, block, ssem.at[3], kvr.at[g, chip], ep=2 * to + core).start()
+        remote(block, block, ssem.at[3], kvr.at[g, kind], ep=2 * to + core).start()
 
     def kv_mate(g, chip):
         block = kv.at[g, core, chip]
         remote(block, block, ssem.at[2], kvm.at[g], ep=mate).start()
 
-    for v_load in v_loads:
-        v_load.wait()
+    loaded(5, kv.at[0, 0, pl.ds(0, kv_here // 2)])
 
     def receive(i):
-        wait_in(xq.at[t, order[i]], zr.at[order[i]])
+        kind = 0
+        if i > 1:
+            for_inner, for_end = ((3, 1), (4, 2), (1, 5), (2, 6), (5, 3), (6, 4))[i - 2]
+            kind = jnp.where(inner, for_inner, for_end)
+        wait_in(xq.at[t, order[i]], zr.at[kind])
         spread(i)
 
     receive(1)
-    q_load.wait()
-    qg_load.wait()
+    loaded(6, q_ref)
     for h in range(kv_here * group):
         qrot[h] = turn(q_ref[:, h * head_dim : (h + 1) * head_dim], qg_ref[...])
     q_of = lambda g: qrot.at[pl.ds(g * group, group)]
 
     def gate_up(q, k, first=False):
-        block = xq[q, pl.ds(base[k], half)].astype(f32).reshape(half * cap, slab).astype(bf16)
+        pieces = [xq[q, pl.ds(2 * chip, 2)].astype(f32).reshape(2 * cap, slab) for chip in sides_of[k]]
+        block = jnp.concatenate(pieces, axis=0).astype(bf16)
         at = pl.ds(pl.multiple_of(q * slab, slab), slab)
-        g = lax.dot_general(block, wg[:, at], (((1,), (1,)), ((), ())), preferred_element_type=f32)
-        u = lax.dot_general(block, wu[:, at], (((1,), (1,)), ((), ())), preferred_element_type=f32)
+        g = lax.dot_general(block, wgu[0, :, at], (((1,), (1,)), ((), ())), preferred_element_type=f32)
+        u = lax.dot_general(block, wgu[1, :, at], (((1,), (1,)), ((), ())), preferred_element_type=f32)
         if first:
             gacc[k] = g
             uacc[k] = u
@@ -433,23 +429,25 @@
         at = pl.ds(pl.multiple_of(q * slab, slab), slab)
         out = jnp.dot(hid[k], wd[:, at], preferred_element_type=f32)
         for s in range(half):
-            part[q, base[k] + s] = out[s * cap : (s + 1) * cap].astype(bf16)
-
-    def rx_copy(s):
-        remote(part.at[tx, s], rs.at[0, s], ssem.at[6], rsr.at[s], tp=tx).start()
-
-    def ry_copy(s):
-        remote(part.at[ty, s], rs.at[1, s], ssem.at[6], rsr.at[s], tp=ty).start()
+            part[q, 2 * sides_of[k][s // 2] + s % 2] = out[s * cap : (s + 1) * cap].astype(bf16)
+
+    def rx_copy(k, j):
+        s = turns[k][j]
+        remote(part.at[tx, s], rs.at[0, s], ssem.at[6], rsr.at[k, j // 2], tp=tx).start()
+
+    def ry_copy(k, j):
+        s = turns[k][j]
+        remote(part.at[ty, s], rs.at[1, s], ssem.at[6], rsr.at[k, j // 2], tp=ty).start()
 
     def send_far(k):
         for j, s in enumerate(turns[k]):
-            remote(part.at[td, s], rdiag.at[s], ssem.at[6], rdr.at[s], tp=tx if j % 2 == 0 else ty).start()
+            to = tx if j % 2 == 0 else ty
+            remote(part.at[td, s], rdiag.at[s], ssem.at[6], rdr.at[k, j // 2], tp=to).start()
 
     def send_near(k):
-        for s in turns[k][0::2]:
-            rx_copy(s)
-        for s in turns[k][1::2]:
-            ry_copy(s)
+        for j in range(0, half, 2):
+            rx_copy(k, j)
+            ry_copy(k, j + 1)
 
     def corner_far(k):
         corner(k)
@@ -468,15 +466,14 @@
     @pl.when(~inner)
     def _():
         for g in range(kv_here):
-            kv_send(g, z, partner)
+            kv_send(g, z, partner, 0)
         for g in range(kv_here):
-            remote(q_of(g), qship.at[g], ssem.at[3], qsr.at[g], ep=2 * partner + core).start()
+            remote(q_of(g), qship.at[g], ssem.at[3], qar.at[g], ep=2 * partner + core).start()
 
     forward(0)
     forward(1)
 
-    wg_load.wait()
-    wu_load.wait()
+    loaded(8, wgu)
 
     @pl.when(~inner)
     def _():
@@ -489,7 +486,7 @@
 
     @pl.when(inner)
     def _():
-        kv_send(0, z, other)
+        kv_send(0, z, other, 1)
         kv_mate(0, z)
         gate_up(t, 0, True)
         forward(2)
@@ -502,24 +499,21 @@
         @pl.when(inner)
         def _():
             for g in heads:
-                kv_send(g, z, other)
+                kv_send(g, z, other, 1)
                 kv_mate(g, z)
 
-    def relay_kv(heads, source, on):
+    def relay_kv(heads, source, kind):
         @pl.when(inner)
         def _():
             for g in heads:
                 block = kv.at[g, core, source]
-                wait_in(block, kvr.at[g, source])
-                if on:
-                    kv_send(g, source, other)
+                wait_in(block, kvr.at[g, kind])
+                if kind == 0:
+                    kv_send(g, source, other, 2)
                 kv_mate(g, source)
 
     own_kv((1,))
     scale = head_dim ** (-0.5) * 1.4426950408889634
-    share = tokens // 4
-    width = wo.shape[1]
-    chunk = width // 4
 
     def attend_one(g, q2):
         keys = kv[g, :, :, 0].reshape(n_ep * tokens, head_dim)
@@ -536,24 +530,25 @@
         @pl.when(inner)
         def _():
             for g in heads:
-                wait_in(qship.at[g], qsr.at[g])
+                wait_in(qship.at[g], qar.at[g])
                 wait_in(kv.at[g, 1 - core], kvm.at[g])
                 aship[g] = attend_one(g, qship[g])
-                remote(aship.at[g], att.at[g], ssem.at[3], atr.at[g], ep=2 * partner + core).start()
+                remote(aship.at[g], att.at[g], ssem.at[3], qar.at[kv_here - 1 if g == kv_here - 1 else 0], ep=2 * partner + core).start()
 
     def meet(k):
         for j, s in enumerate(turns[k]):
-            wait_in(rdiag.at[s], rdr.at[s])
             if j % 2 == 0:
+                wait_in(rdiag.at[pl.ds(0, 2)], rdr.at[k, j // 2])
                 part[ty, s] = (part[ty, s].astype(f32) + rdiag[s].astype(f32)).astype(bf16)
-                ry_copy(s)
+                ry_copy(k, j)
             else:
                 part[tx, s] = (part[tx, s].astype(f32) + rdiag[s].astype(f32)).astype(bf16)
-                rx_copy(s)
+                rx_copy(k, j)
 
     def finish(k):
         for j, s in enumerate(turns[k]):
-            wait_in(rs.at[0, pl.ds(0, 2)], rsr.at[s])
+            if j % 2 == 0:
+                wait_in(rs.at[0, pl.ds(0, 4)], rsr.at[k, j // 2])
             out = (part[t, s].astype(f32) + rs[0, s].astype(f32) + rs[1, s].astype(f32)).astype(bf16)
             if k == 0 and j == half - 1:
                 ret[s] = out
@@ -562,10 +557,9 @@
                 remote(back.at[s], ret.at[me], ssem.at[7], br.at[0], ep=s).start()
 
     share = tokens // 4
-    width = wo.shape[1]
     chunk = width // 4
 
-    wd_load.wait()
+    loaded(9, wd)
     sides(0)
     gate_up(tx, 0)
     gate_up(ty, 0)
@@ -574,47 +568,49 @@
     def _():
         corner_far(0)
         down_rest(0)
+        send_far(0)
 
     forward(4)
     forward(5)
-    relay_kv((0,), partner, True)
+    relay_kv((0,), partner, 0)
     own_kv((2,))
 
     @pl.when(inner)
     def _():
         corner_far(0)
-
-    send_far(0)
+        send_far(0)
+
     forward(6)
     forward(7)
-    relay_kv((1,), partner, True)
+    relay_kv((1,), partner, 0)
     own_kv((3,))
-    relay_kv((0, 1), other, False)
+    relay_kv((0, 1), other, 1)
 
     @pl.when(inner)
     def _():
         down_rest(0)
 
     send_near(0)
-    relay_kv((2, 3), partner, True)
-    relay_kv((0,), far_end, False)
+    relay_kv((2, 3), partner, 0)
+    relay_kv((0,), far_end, 2)
     gate_up(t, 1, True)
     sides(1)
     gate_up(tx, 1)
     gate_up(ty, 1)
+    meet(0)
     attend_ship((0,))
-    relay_kv((2,), other, False)
-    relay_kv((1,), far_end, False)
+    relay_kv((2,), other, 1)
+    relay_kv((1,), far_end, 2)
     corner_far(1)
     send_far(1)
     down_rest(1)
     send_near(1)
-    meet(0)
     attend_ship((1,))
-    relay_kv((3,), other, False)
-    relay_kv((2,), far_end, False)
-    relay_kv((3,), far_end, False)
+    relay_kv((3,), other, 1)
+    relay_kv((2,), far_end, 2)
+    relay_kv((3,), far_end, 2)
     attend_ship((2, 3))
+    finish(0)
     meet(1)
 
     @pl.when(inner)
@@ -622,22 +618,23 @@
         for g in range(kv_here):
             att[g] = attend_one(g, qrot[g * group : (g + 1) * group])
 
-    finish(0)
-    finish(1)
-
-
-    def attended(heads):
+
+    @pl.when(inner)
+    def _():
+        finish(1)
+
+
+    def attended(first, count, i):
         @pl.when(~inner)
         def _():
-            for g in heads:
-                wait_in(att.at[g], atr.at[g])
-
-    attended(range(kv_here - 1))
-    wo_load.wait()
+            wait_in(att.at[pl.ds(first, count)], qar.at[i])
+
+    attended(0, kv_here - 1, 0)
+    loaded(10, wo)
     cut = (kv_here - 1) * group * head_dim
     early = jnp.concatenate([att[g] for g in range(kv_here - 1)], axis=1)
     macc[...] = jnp.dot(early, wo[:cut, :], preferred_element_type=f32)
-    attended((kv_here - 1,))
+    attended(kv_here - 1, 1, kv_here - 1)
     for c in range(4):
         at = slice(c * chunk, (c + 1) * chunk)
         out = macc[:, at] + jnp.dot(att[kv_here - 1], wo[cut:, at], preferred_element_type=f32)
@@ -646,7 +643,11 @@
         for i, to in enumerate((td, tx, ty)):
             remote(mpart.at[c, to], mrecv.at[c, i], ssem.at[5], mr.at[c], tp=to).start()
 
-    lg_load.wait()
+    @pl.when(~inner)
+    def _():
+        finish(1)
+
+    loaded(7, lg_ref)
     ids = rt_ref[...].astype(f32)
     logits = lg_ref[...]
     stacked = jnp.where(
@@ -758,14 +759,11 @@
             pltpu.VMEM(queries.shape, bf16),
             pltpu.VMEM(keys.shape, bf16),
             pltpu.VMEM(expert_input.shape, bf16),
-            pltpu.VMEM((1, head_dim), f32),
-            pltpu.VMEM((1, head_dim), f32),
-            pltpu.VMEM((1, width), f32),
+            pltpu.VMEM((1, width + 2 * head_dim), f32),
             pltpu.VMEM((2, tokens), jnp.int32),
             pltpu.VMEM((2, tokens), f32),
             pltpu.VMEM(out_weight.shape, bf16),
-            pltpu.VMEM((ff, width), bf16),
-            pltpu.VMEM((ff, width), bf16),
+            pltpu.VMEM((2, ff, width), bf16),
             pltpu.VMEM(down_weight.shape[1:], bf16),
             pltpu.VMEM((2, tokens, head_dim), f32),
             pltpu.VMEM(piece, bf16),
@@ -786,18 +784,17 @@
             pltpu.VMEM((tokens, width), f32),
             pltpu.VMEM((4, n_tp, share, chunk), bf16),
             pltpu.VMEM((4, 3, share, chunk), bf16),
-            dma((13 + kv_here,)),
+            dma((11,)),
             dma((8,)),
-            dma((n_ep,)),
+            dma((7,)),
             dma((n_ep // 2 + 2,)),
             dma((n_ep // 2 + 2,)),
             dma((2,)),
-            dma((kv_here, n_ep // 2)),
+            dma((kv_here, 3)),
             dma((kv_here,)),
             dma((kv_here,)),
-            dma((kv_here,)),
-            dma((n_ep,)),
-            dma((n_ep,)),
+            dma((2, 2)),
+            dma((2, 2)),
             dma((1,)),
             dma((4,)),
         ],

time: 42.3 us -> 41.6 us (0.983)
  Pallas kernels: 41.5 us -> 40.8 us
    pallas_call x1, Pallas kernels: 40.8 us -> 40.1 us  [kernel_form(): pl.pallas_call(functools.partial(fused, dims), name='fused', out_shape=(p...]
where the time goes in v5:
time: 41.6 us; the launch traced here: 41.4 us
  Pallas kernels  40.8 us (98%)
  between operations  0.64 us (2%)
    pallas_call x1, Pallas kernels, kernel_form(): pl.pallas_call(functools.partial(fused, dims), name='fused', out_shape=(p...  40.1 us

profile of v5, /device:TPU:0, one launch (start us, length us, event | category | flops | bytes accessed | tf_op | source)
XLA Modules:
  0.0 41.4 jit_solution(12945149662411613030)
XLA Ops:
  0.6 40.1 %fused.1 = (bf16[32,2048]{1,0:T(8,128)(2,1)S(1)}, bf16[128,512]{1,0:T(8,128)(2,1)S(1)}) custom-call(bf16[128,1024]{1,0:T(8,128)(2,1)} %q_hbm.1, bf16[128,512]{1,0:T(8,128)(2,1)} %k_hbm.1, bf16[128,512]{1,0:T(8,128)(2,1)} %v_hbm.1, f32[1,128]{1,0:T(1,128)} %bitcast.12, f32[1,128]{1,0:T(1,128)} %bitcast.13, bf16[1024,2048]{1,0:T(8,128)(2,1)} %wo_hbm.1, ...), custom_call_target="tpu_custom_call" | custom-call | tf_op jit(solution)/shard_map/fused/pallas_call | solution.py:749
  40.7 0.7 %hand_over.1 = (bf16[32,2048]{1,0:T(8,128)(2,1)}, bf16[128,512]{1,0:T(8,128)(2,1)}) custom-call(bf16[32,2048]{1,0:T(8,128)(2,1)S(1)} %get-tuple-element.4.a_ref, bf16[128,512]{1,0:T(8,128)(2,1)S(1)} %get-tuple-element.5.b_ref), custom_call_target="tpu_custom_call" | custom-call | tf_op jit(solution)/shard_map/hand_over/pallas_call | solution.py:820

commit v6 on v5

--- a/solution.py
+++ b/solution.py
@@ -226,6 +226,7 @@
     aship,
     macc,
     mpart,
+    mfar,
     mrecv,
     wsem,
     ssem,
@@ -239,6 +240,7 @@
     rdr,
     rsr,
     br,
+    mf,
     mr,
 ):
     n_ep, cap, head_dim, kv_here, group = dims
@@ -635,13 +637,21 @@
     early = jnp.concatenate([att[g] for g in range(kv_here - 1)], axis=1)
     macc[...] = jnp.dot(early, wo[:cut, :], preferred_element_type=f32)
     attended(kv_here - 1, 1, kv_here - 1)
-    for c in range(4):
+    def m_send(a, b, sem, to):
+        remote(a, b, ssem.at[5], sem, tp=to).start()
+
+    for c in (0, 2, 1, 3):
         at = slice(c * chunk, (c + 1) * chunk)
         out = macc[:, at] + jnp.dot(att[kv_here - 1], wo[cut:, at], preferred_element_type=f32)
         for j in range(4):
             mpart[c, j] = out[j * share : (j + 1) * share].astype(bf16)
-        for i, to in enumerate((td, tx, ty)):
-            remote(mpart.at[c, to], mrecv.at[c, i], ssem.at[5], mr.at[c], tp=to).start()
+        if c % 2 == 0:
+            to = tx if c == 0 else ty
+            m_send(mpart.at[c, td], mfar.at[c // 2], mf.at[c // 2], to)
+            m_send(mpart.at[c, to], mrecv.at[c, c // 2], mr.at[c], to)
+        else:
+            for i, to in ((2, td), (0, tx), (1, ty)):
+                m_send(mpart.at[c, to], mrecv.at[c, i], mr.at[c], to)
 
     @pl.when(~inner)
     def _():
@@ -673,15 +683,22 @@
     l1 = columns[:, 3:4]
     w0 = jax.nn.sigmoid(l0 - l1)
     w1 = jax.nn.sigmoid(l1 - l0)
+    for c in (0, 2):
+        to = ty if c == 0 else tx
+        wait_in(mfar.at[c // 2], mf.at[c // 2])
+        mpart[c, to] = (mpart[c, to].astype(f32) + mfar[c // 2].astype(f32)).astype(bf16)
+        m_send(mpart.at[c, to], mrecv.at[c, 1 - c // 2], mr.at[c], to)
+
     wait_in(ret.at[pl.ds(0, n_ep - 1)], br.at[0])
     results = ret[...].astype(f32).reshape(rows, slab).astype(bf16)
     first = jnp.dot(c0, results, preferred_element_type=f32)
     second = jnp.dot(c1, results, preferred_element_type=f32)
     eout_ref[...] = (w0 * first + w1 * second).astype(bf16)
-    for c in range(4):
-        wait_in(mrecv.at[c], mr.at[c])
+    for c in (1, 3, 0, 2):
+        count = 2 + c % 2
+        wait_in(mrecv.at[c, pl.ds(0, count)], mr.at[c])
         summed = mpart[c, t].astype(f32)
-        for i in range(3):
+        for i in range(count):
             summed = summed + mrecv[c, i].astype(f32)
         mixed_ref[:, c * chunk : (c + 1) * chunk] = summed.astype(bf16)
 
@@ -783,6 +800,7 @@
             pltpu.VMEM((kv_here, tokens, heads // kv_here * head_dim), bf16),
             pltpu.VMEM((tokens, width), f32),
             pltpu.VMEM((4, n_tp, share, chunk), bf16),
+            pltpu.VMEM((2, share, chunk), bf16),
             pltpu.VMEM((4, 3, share, chunk), bf16),
             dma((11,)),
             dma((8,)),
@@ -796,6 +814,7 @@
             dma((2, 2)),
             dma((2, 2)),
             dma((1,)),
+            dma((2,)),
             dma((4,)),
         ],
         compiler_params=pltpu.CompilerParams(

time: 41.6 us -> 40.9 us (0.983)
  Pallas kernels: 40.8 us -> 40.1 us
    pallas_call x1, Pallas kernels: 40.1 us -> 39.4 us  [kernel_form(): pl.pallas_call(functools.partial(fused, dims), name='fused', out_shape=(p...]
where the time goes in v6:
time: 40.9 us; the launch traced here: 40.7 us
  Pallas kernels  40.1 us (98%)
  between operations  0.64 us (2%)
    pallas_call x1, Pallas kernels, kernel_form(): pl.pallas_call(functools.partial(fused, dims), name='fused', out_shape=(p...  39.4 us

profile of v6, /device:TPU:0, one launch (start us, length us, event | category | flops | bytes accessed | tf_op | source)
XLA Modules:
  0.0 40.7 jit_solution(5026105760438263888)
XLA Ops:
  0.6 39.4 %fused.1 = (bf16[32,2048]{1,0:T(8,128)(2,1)S(1)}, bf16[128,512]{1,0:T(8,128)(2,1)S(1)}) custom-call(bf16[128,1024]{1,0:T(8,128)(2,1)} %q_hbm.1, bf16[128,512]{1,0:T(8,128)(2,1)} %k_hbm.1, bf16[128,512]{1,0:T(8,128)(2,1)} %v_hbm.1, f32[1,128]{1,0:T(1,128)} %bitcast.12, f32[1,128]{1,0:T(1,128)} %bitcast.13, bf16[1024,2048]{1,0:T(8,128)(2,1)} %wo_hbm.1, ...), custom_call_target="tpu_custom_call" | custom-call | tf_op jit(solution)/shard_map/fused/pallas_call | solution.py:766
  40.0 0.7 %hand_over.1 = (bf16[32,2048]{1,0:T(8,128)(2,1)}, bf16[128,512]{1,0:T(8,128)(2,1)}) custom-call(bf16[32,2048]{1,0:T(8,128)(2,1)S(1)} %get-tuple-element.4.a_ref, bf16[128,512]{1,0:T(8,128)(2,1)S(1)} %get-tuple-element.5.b_ref), custom_call_target="tpu_custom_call" | custom-call | tf_op jit(solution)/shard_map/hand_over/pallas_call | solution.py:839

commit v7 on v6

--- a/solution.py
+++ b/solution.py
@@ -691,9 +691,8 @@
 
     wait_in(ret.at[pl.ds(0, n_ep - 1)], br.at[0])
     results = ret[...].astype(f32).reshape(rows, slab).astype(bf16)
-    first = jnp.dot(c0, results, preferred_element_type=f32)
-    second = jnp.dot(c1, results, preferred_element_type=f32)
-    eout_ref[...] = (w0 * first + w1 * second).astype(bf16)
+    both = jnp.dot(jnp.concatenate([c0, c1], axis=0), results, preferred_element_type=f32)
+    eout_ref[...] = (w0 * both[:tokens] + w1 * both[tokens:]).astype(bf16)
     for c in (1, 3, 0, 2):
         count = 2 + c % 2
         wait_in(mrecv.at[c, pl.ds(0, count)], mr.at[c])

time: 40.9 us -> 40.9 us (level)
  no operation moved by 1% of the time
where the time goes in v7:
time: 40.9 us; the launch traced here: 40.7 us
  Pallas kernels  40.1 us (98%)
  between operations  0.64 us (2%)
    pallas_call x1, Pallas kernels, kernel_form(): pl.pallas_call(functools.partial(fused, dims), name='fused', out_shape=(p...  39.4 us

profile of v7, /device:TPU:0, one launch (start us, length us, event | category | flops | bytes accessed | tf_op | source)
XLA Modules:
  0.0 40.7 jit_solution(6534007916423370491)
XLA Ops:
  0.6 39.4 %fused.1 = (bf16[32,2048]{1,0:T(8,128)(2,1)S(1)}, bf16[128,512]{1,0:T(8,128)(2,1)S(1)}) custom-call(bf16[128,1024]{1,0:T(8,128)(2,1)} %q_hbm.1, bf16[128,512]{1,0:T(8,128)(2,1)} %k_hbm.1, bf16[128,512]{1,0:T(8,128)(2,1)} %v_hbm.1, f32[1,128]{1,0:T(1,128)} %bitcast.12, f32[1,128]{1,0:T(1,128)} %bitcast.13, bf16[1024,2048]{1,0:T(8,128)(2,1)} %wo_hbm.1, ...), custom_call_target="tpu_custom_call" | custom-call | tf_op jit(solution)/shard_map/fused/pallas_call | solution.py:765
  40.0 0.7 %hand_over.1 = (bf16[32,2048]{1,0:T(8,128)(2,1)}, bf16[128,512]{1,0:T(8,128)(2,1)}) custom-call(bf16[32,2048]{1,0:T(8,128)(2,1)S(1)} %get-tuple-element.4.a_ref, bf16[128,512]{1,0:T(8,128)(2,1)S(1)} %get-tuple-element.5.b_ref), custom_call_target="tpu_custom_call" | custom-call | tf_op jit(solution)/shard_map/hand_over/pallas_call | solution.py:838
